TPU v7x, 256 devices: a whole 4x4x8 slice. The times are simulated.
256 devices in a mesh: kv: 32 (over z, y), tp: 8 (over x, core).
Axes of the slice: x: 4, y: 4, z: 8, core: 2. Of those that a mesh axis runs over, the one named last changes fastest.
Arguments:
- stream: bfloat16 [128, 4096], P(None, ('kv', 'tp')), may hold values from -60 to 60
- memory_state: float32 [128, 32, 128, 128], P('kv', 'tp'), may hold values from -3 to 3
- attn_gain: float32 [4096], P('kv'), may hold values from 0.1 to 1.9
- query_weight: bfloat16 [4096, 4096], P('kv', 'tp'), may hold values from -0.09375 to 0.09375
- key_weight: bfloat16 [4096, 4096], P('kv', 'tp'), may hold values from -0.09375 to 0.09375
- value_weight: bfloat16 [4096, 4096], P('kv', 'tp'), may hold values from -0.09375 to 0.09375
- outgate_weight: bfloat16 [4096, 4096], P('kv', 'tp'), may hold values from -0.09375 to 0.09375
- beta_weight: bfloat16 [4096, 32], P('kv', 'tp'), may hold values from -0.09375 to 0.09375
- decay_weight: bfloat16 [4096, 32], P('kv', 'tp'), may hold values from -0.09375 to 0.09375
- decay_log: float32 [32], P('tp'), may hold values from -4 to 1
- decay_shift: float32 [32], P('tp'), may hold values from -3 to 3
- head_gain: float32 [128], replicated, may hold values from 0.1 to 1.9
- output_weight: bfloat16 [4096, 4096], P('tp', 'kv'), may hold values from -0.09375 to 0.09375
- mixer_gain: float32 [4096], P('kv'), may hold values from 0.1 to 1.9
- up_weight: bfloat16 [4096, 16384], P('kv', 'tp'), may hold values from -0.09375 to 0.09375
- down_weight: bfloat16 [16384, 4096], P('tp', 'kv'), may hold values from -0.046875 to 0.046875
Outputs:
- layer_out: bfloat16 [128, 4096], P(None, ('kv', 'tp'))
- memory_next: float32 [128, 32, 128, 128], P('kv', 'tp')
All inputs are finite; a program needn't handle non-finite values.
Results may differ from a plain program's by a relative error of at most 0.025.
Values may be sent and summed in bfloat16 or wider, within the bound.
A program may use at most 64 MiB of HBM per device.

v0:
```python
import jax
import jax.numpy as jnp
from jax import lax
from jax.sharding import PartitionSpec as P

D = 4096
HEAD_DIM = 128


epsilon = 1e-06


def split_up(value, dim, length):
    dims = value.shape
    pieces = value.reshape(*dims[:dim], length, dims[dim] // length, *dims[dim + 1 :])
    return jnp.moveaxis(pieces, dim, 0)


def sent_and_summed(value, axis, dim):
    length = lax.axis_size(axis)
    pieces = lax.all_to_all(split_up(value, dim, length), axis, 0, 0, tiled=True)
    return jnp.sum(pieces.astype(jnp.float32), axis=0)


def side_by_side(arrays, axis, dim, along):
    columns = [a.reshape(*a.shape[:along], -1) for a in arrays]
    both = jnp.concatenate(columns, axis=along)
    out, at, gathered = (sent_and_summed(both, axis, dim), 0, [])
    for a, column in zip(arrays, columns):
        share = out[..., at : at + column.shape[along]]
        gathered.append(share.reshape(*share.shape[:along], *a.shape[along:]))
        at += column.shape[along]
    return tuple(gathered)


def joined_along(pieces, dim):
    dims = list(pieces.shape[1:])
    dims[dim] *= pieces.shape[0]
    return jnp.moveaxis(pieces, 0, dim).reshape(dims)


def copy_for_each(value, axis):
    copies = jnp.broadcast_to(value, (lax.axis_size(axis), *value.shape))
    return lax.all_to_all(copies, axis, split_axis=0, concat_axis=0, tiled=True)


def collect(value, axis, dim):
    return joined_along(copy_for_each(value, axis), dim)


def sent_and_summed_2(value, axis, dim):
    pieces = split_up(value, dim, lax.axis_size(axis))
    arrived = lax.all_to_all(pieces, axis, split_axis=0, concat_axis=0, tiled=True)
    return arrived.sum(axis=0)


def gathered_rows(stream, gain_vec):
    gathered = lax.all_gather(stream, "tp", axis=1, tiled=True)
    widened = gathered.astype(jnp.float32)
    squares = jnp.sum(widened * widened, axis=1)
    scaled = (widened * gain_vec).astype(jnp.bfloat16)
    return (scaled, squares)


def unit_rows(values):
    return values * lax.rsqrt(jnp.sum(values * values, axis=-1, keepdims=True) + epsilon)


def head_output(
    memory_state,
    query_sum,
    key_sum,
    value_sum,
    gate_sum,
    beta_sum,
    decay_sum,
    decay_log,
    decay_shift,
    head_gain,
):
    row_count = query_sum.shape[0]
    head_count = beta_sum.shape[1]

    def to_heads(values):
        return values.reshape(row_count, head_count, HEAD_DIM)

    query_heads = unit_rows(jax.nn.silu(to_heads(query_sum))) * HEAD_DIM ** (-0.5)
    key_heads = unit_rows(jax.nn.silu(to_heads(key_sum)))
    value_heads = jax.nn.silu(to_heads(value_sum))
    beta_heads = jax.nn.sigmoid(beta_sum)
    decay_heads = jnp.exp(-jnp.exp(decay_log) * jax.nn.softplus(decay_sum + decay_shift))
    kept_state = memory_state * decay_heads[:, :, None, None]
    recalled = jnp.einsum("bhkv,bhk->bhv", kept_state, key_heads)
    correction = beta_heads[:, :, None] * (value_heads - recalled)
    memory_next = kept_state + key_heads[:, :, :, None] * correction[:, :, None, :]
    readout = jnp.einsum("bhkv,bhk->bhv", memory_next, query_heads)
    normed = readout * lax.rsqrt(jnp.mean(readout * readout, axis=-1, keepdims=True) + epsilon)
    gated = normed * head_gain * jax.nn.silu(to_heads(gate_sum))
    return (gated.reshape(row_count, head_count * HEAD_DIM).astype(jnp.bfloat16), memory_next)


def shards(
    stream,
    memory_state,
    attn_gain,
    query_weight,
    key_weight,
    value_weight,
    outgate_weight,
    beta_weight,
    decay_weight,
    decay_log,
    decay_shift,
    head_gain,
    output_weight,
    mixer_gain,
    up_weight,
    down_weight,
):
    scaled, squares = gathered_rows(stream, attn_gain)

    def product(weight):
        return jnp.dot(scaled, weight, preferred_element_type=jnp.float32)

    query_sum, key_sum, value_sum, gate_sum, beta_sum, decay_sum, own_squares = side_by_side(
        (
            product(query_weight).astype(jnp.bfloat16),
            product(key_weight).astype(jnp.bfloat16),
            product(value_weight).astype(jnp.bfloat16),
            product(outgate_weight).astype(jnp.bfloat16),
            product(beta_weight).astype(jnp.bfloat16),
            product(decay_weight).astype(jnp.bfloat16),
            squares.astype(jnp.bfloat16),
        ),
        "kv",
        0,
        1,
    )
    factor = lax.rsqrt(own_squares / D + epsilon)[:, None]
    heads_out, memory_next = head_output(
        memory_state,
        query_sum * factor,
        key_sum * factor,
        value_sum * factor,
        gate_sum * factor,
        beta_sum * factor,
        decay_sum * factor,
        decay_log,
        decay_shift,
        head_gain,
    )
    attn_rows = jnp.dot(
        collect(heads_out, "kv", 0), output_weight, preferred_element_type=jnp.float32
    )
    attn_mine = sent_and_summed_2(attn_rows, "tp", 1)
    middle = (stream.astype(jnp.float32) + attn_mine).astype(jnp.bfloat16)
    scaled_mix, squares_mix = gathered_rows(middle, mixer_gain)
    up_part = jnp.dot(scaled_mix, up_weight, preferred_element_type=jnp.float32)
    up_mine, square_mine = side_by_side(
        (up_part.astype(jnp.bfloat16), squares_mix.astype(jnp.bfloat16)), "kv", 0, 1
    )
    hidden = jnp.square(
        jax.nn.relu(up_mine * lax.rsqrt(square_mine / D + epsilon)[:, None])
    ).astype(jnp.bfloat16)
    down_rows = jnp.dot(collect(hidden, "kv", 0), down_weight, preferred_element_type=jnp.float32)
    mixer_mine = lax.psum_scatter(
        down_rows.astype(jnp.bfloat16), "tp", scatter_dimension=1, tiled=True
    ).astype(jnp.float32)
    layer_out = (middle.astype(jnp.float32) + mixer_mine).astype(jnp.bfloat16)
    return (layer_out, memory_next)


def solution(mesh):
    in_specs = (
        P(None, ("kv", "tp")),
        P("kv", "tp", None, None),
        P("kv"),
        P("kv", "tp"),
        P("kv", "tp"),
        P("kv", "tp"),
        P("kv", "tp"),
        P("kv", "tp"),
        P("kv", "tp"),
        P("tp"),
        P("tp"),
        P(),
        P("tp", "kv"),
        P("kv"),
        P("kv", "tp"),
        P("tp", "kv"),
    )
    out_specs = (P(None, ("kv", "tp")), P("kv", "tp", None, None))
    return jax.shard_map(shards, mesh=mesh, in_specs=in_specs, out_specs=out_specs, check_vma=False)
```

profile of v0, /device:TPU:1, one launch (start us, length us, event | category | flops | bytes accessed | tf_op | source)
XLA Modules:
  0.0 181.2 jit_solution(9769738742397507875)
XLA Ops:
  7.2 16.2 %all_gather.6 = bf16[128,128]{0,1:T(8,128)(2,1)S(1)} all-gather(bf16[128,16]{0,1:T(8,128)(2,1)} %param.16), channel_id=1, replica_groups=mesh['kv'=32,'tp'=8] {'tp'}, dimensions={1}, use_global_device_ids=true | all-gather | bytes 36864 | tf_op jit(solution)/shard_map/all_gather | solution.py:58
  23.5 0.9 convolution_convert_fusion.7
  24.4 0.9 convolution_convert_fusion.6
  25.2 0.1 copy.65
  25.4 0.1 copy.64
  25.5 0.2 convert_element_type.120
  25.8 1.2 convolution_convert_fusion.3
  27.0 1.2 convolution_convert_fusion.2
  28.3 0.3 convolution_convert_fusion.1
  28.6 0.3 convolution_convert_fusion.4
  29.0 2.0 %concatenate.28 = bf16[32,4,2057]{2,1,0:T(4,128)(2,1)} concatenate(bf16[32,4,512]{2,1,0:T(4,128)(2,1)S(1)} %concatenate.22, bf16[32,4,512]{2,1,0:T(4,128)(2,1)S(1)} %concatenate.23, bf16[32,4,512]{2,1,0:T(4,128)(2,1)S(1)} %concatenate.24, bf16[32,4,512]{2,1,0:T(4,128)(2,1)S(1)} %concatenate.25, bf16[32,4,4]{2,1,0:T(4,128)(2,1)S(1)} %bitcast.38, bf16[32,4,4]{2,1,0:T(4,128)(2,1)S(1)} %bitcast.37, ...), dimensions={2} | concatenate | bytes 1053184 | tf_op jit(solution)/shard_map/concatenate | solution.py:27
  31.0 10.0 %all-to-all-start = ((bf16[32,4,2057]{2,1,0:T(4,128)(2,1)}), bf16[32,4,2057]{2,1,0:T(4,128)(2,1)S(1)}, u32[]{:S(2)}, u32[]{:S(2)}) async-start(bf16[32,4,2057]{2,1,0:T(4,128)(2,1)} %concatenate.28), calls=%async_computation | async-start | bytes 1114112 | tf_op jit(solution)/shard_map/all_to_all | solution.py:21
  41.0 17.2 %all-to-all-done = bf16[32,4,2057]{2,1,0:T(4,128)(2,1)S(1)} async-done(((bf16[32,4,2057]{2,1,0:T(4,128)(2,1)}), bf16[32,4,2057]{2,1,0:T(4,128)(2,1)S(1)}, u32[]{:S(2)}, u32[]{:S(2)}) %all-to-all-start) | async-done | bytes 526624 | tf_op jit(solution)/shard_map/all_to_all | solution.py:21
  58.2 0.2 convert_reduce_fusion.1
  58.5 0.2 fusion.28
  58.7 0.1 slice_multiply_fusion.2
  58.8 0.1 multiply_reduce_fusion.1
  58.9 0.1 multiply_multiply_fusion
  59.0 0.1 multiply_reduce_fusion.2
  59.1 0.1 broadcast_multiply_fusion
  59.2 0.1 fusion.25
  59.3 0.3 fusion
  59.6 0.1 fusion.14
  59.7 0.4 multiply_add_fusion
  60.1 0.2 fusion.36
  60.4 0.1 multiply_reduce_fusion
  60.5 0.3 copy-done.11
  60.9 0.7 broadcast_in_dim.4
  61.5 5.2 %all-to-all-start.1 = ((bf16[32,4,512]{2,1,0:T(4,128)(2,1)}), bf16[32,4,512]{2,1,0:T(4,128)(2,1)S(1)}, u32[]{:S(2)}, u32[]{:S(2)}) async-start(bf16[32,4,512]{2,1,0:T(4,128)(2,1)} %broadcast_in_dim.4), calls=%async_computation.1 | async-start | bytes 262144 | tf_op jit(solution)/shard_map/all_to_all | solution.py:44
  66.8 0.1 copy.58
  66.9 9.2 %all-to-all-done.1 = bf16[32,4,512]{2,1,0:T(4,128)(2,1)S(1)} async-done(((bf16[32,4,512]{2,1,0:T(4,128)(2,1)}), bf16[32,4,512]{2,1,0:T(4,128)(2,1)S(1)}, u32[]{:S(2)}, u32[]{:S(2)}) %all-to-all-start.1) | async-done | bytes 131104 | tf_op jit(solution)/shard_map/all_to_all | solution.py:44
  76.1 0.2 convolution_bitcast_fusion
  76.3 11.1 %all_to_all.25 = f32[8,128,16]{1,2,0:T(8,128)S(1)} all-to-all(f32[8,128,16]{1,2,0:T(8,128)S(1)} %convolution_bitcast_fusion), channel_id=1, replica_groups=mesh['kv'=32,'tp'=8] {'tp'}, dimensions={0} | all-to-all | bytes 131072 | tf_op jit(solution)/shard_map/all_to_all | solution.py:53
  87.5 13.5 %all_gather.7 = bf16[128,128]{0,1:T(8,128)(2,1)S(1)} all-gather(bf16[128,16]{0,1:T(8,128)(2,1)S(1)} %add_convert_fusion.1), channel_id=1, replica_groups=mesh['kv'=32,'tp'=8] {'tp'}, dimensions={1}, use_global_device_ids=true | all-gather | bytes 36864 | tf_op jit(solution)/shard_map/all_gather | solution.py:58
  101.0 0.2 convert_element_type.121
  101.3 0.4 convolution_convert_fusion
  101.7 0.2 concatenate.29
  101.9 0.3 pad_maximum_fusion
  102.2 20.2 %all_to_all.26 = bf16[32,4,2049]{2,1,0:T(4,128)(2,1)S(1)} all-to-all(bf16[32,4,2049]{2,1,0:T(4,128)(2,1)S(1)} %pad_maximum_fusion), channel_id=1, replica_groups=mesh['kv'=32,'tp'=8] {'kv'}, dimensions={0} | all-to-all | bytes 1049088 | tf_op jit(solution)/shard_map/all_to_all | solution.py:21
  122.4 0.2 convert_reduce_fusion
  122.6 0.1 fusion.21
  122.7 0.1 fusion.10
  122.8 0.2 broadcast_in_dim.5
  123.1 20.6 %all_to_all.27 = bf16[32,4,2048]{2,1,0:T(4,128)(2,1)S(1)} all-to-all(bf16[32,4,2048]{2,1,0:T(4,128)(2,1)S(1)} %broadcast_in_dim.5), channel_id=1, replica_groups=mesh['kv'=32,'tp'=8] {'kv'}, dimensions={0} | all-to-all | bytes 1048576 | tf_op jit(solution)/shard_map/all_to_all | solution.py:44
  143.7 0.1 reshape.111
  143.8 0.9 convolution_convert_fusion.5
  144.8 28.3 %reduce-scatter.2.cloned.1.call-done = bf16[128,16]{0,1:T(8,128)(2,1)} async-done(((bf16[128,128]{0,1:T(8,128)(2,1)}), bf16[128,16]{0,1:T(8,128)(2,1)}) %reduce-scatter.2.cloned.1.call-update) | async-done | bytes 4112 | tf_op jit(solution)/shard_map/reduce_scatter | solution.py:166
  173.1 1.3 add_convert_fusion
  (46 shorter events, 0.6 us)
Async XLA Ops:
  7.2 94.1 %copy-start = (bf16[128,2048]{1,0:T(8,128)(2,1)S(1)}, bf16[128,2048]{1,0:T(8,128)(2,1)}, u32[]{:S(2)}) copy-start(bf16[128,2048]{1,0:T(8,128)(2,1)} %param.30) | copy-start | bytes 1572868
  7.2 21.1 %copy-start.8 = (f32[128]{0:T(128)S(1)}, f32[128]{0:T(128)}, u32[]{:S(2)}) copy-start(f32[128]{0:T(128)} %param.18) | copy-start | bytes 1540
  7.2 21.1 %copy-start.4 = (bf16[128,512]{1,0:T(8,128)(2,1)S(1)}, bf16[128,512]{1,0:T(8,128)(2,1)}, u32[]{:S(2)}) copy-start(bf16[128,512]{1,0:T(8,128)(2,1)} %param.22) | copy-start | bytes 393220
  7.2 21.4 %copy-start.5 = (bf16[128,512]{1,0:T(8,128)(2,1)S(1)}, bf16[128,512]{1,0:T(8,128)(2,1)}, u32[]{:S(2)}) copy-start(bf16[128,512]{1,0:T(8,128)(2,1)} %param.19) | copy-start | bytes 393220
  28.9 12.0 %copy-start.12 = (f32[4]{0:T(128)S(1)}, f32[4]{0:T(128)}, u32[]{:S(2)}) copy-start(f32[4]{0:T(128)} %param.25) | copy-start | bytes 52
  31.0 28.2 %copy-start.10 = (f32[4]{0:T(128)S(1)}, f32[4]{0:T(128)}, u32[]{:S(2)}) copy-start(f32[4]{0:T(128)} %param.26) | copy-start | bytes 52
  31.0 28.3 %copy-start.1 = (f32[4,4,128,128]{3,2,1,0:T(8,128)S(1)}, f32[4,4,128,128]{3,2,1,0:T(8,128)}, u32[]{:S(2)}) copy-start(f32[4,4,128,128]{3,2,1,0:T(8,128)} %param.17) | copy-start | bytes 3145732
  31.0 27.2 %all-to-all-start = ((bf16[32,4,2057]{2,1,0:T(4,128)(2,1)}), bf16[32,4,2057]{2,1,0:T(4,128)(2,1)S(1)}, u32[]{:S(2)}, u32[]{:S(2)}) async-start(bf16[32,4,2057]{2,1,0:T(4,128)(2,1)} %concatenate.28), calls=%async_computation | async-start | bytes 1114112 | tf_op jit(solution)/shard_map/all_to_all | solution.py:21
  60.1 16.2 %copy-start.2 = (f32[4,4,128,128]{3,2,1,0:T(8,128)}, f32[4,4,128,128]{3,2,1,0:T(8,128)S(1)}, u32[]{:S(2)}) copy-start(f32[4,4,128,128]{3,2,1,0:T(8,128)S(1)} %multiply_add_fusion) | copy-start | bytes 3145732
  60.1 0.7 copy-start.11
  60.1 6.7 %copy-start.6 = (bf16[512,128]{1,0:T(8,128)(2,1)S(1)}, bf16[512,128]{1,0:T(8,128)(2,1)}, u32[]{:S(2)}) copy-start(bf16[512,128]{1,0:T(8,128)(2,1)} %param.28) | copy-start | bytes 393220
  60.1 27.3 %copy-start.7 = (bf16[128,16]{0,1:T(8,128)(2,1)S(1)}, bf16[128,16]{0,1:T(8,128)(2,1)}, u32[]{:S(2)}) copy-start(bf16[128,16]{0,1:T(8,128)(2,1)} %param.16) | copy-start | bytes 12292
  60.4 40.9 %copy-start.9 = (f32[128]{0:T(128)S(1)}, f32[128]{0:T(128)}, u32[]{:S(2)}) copy-start(f32[128]{0:T(128)} %param.29) | copy-start | bytes 1540
  61.5 14.5 %all-to-all-start.1 = ((bf16[32,4,512]{2,1,0:T(4,128)(2,1)}), bf16[32,4,512]{2,1,0:T(4,128)(2,1)S(1)}, u32[]{:S(2)}, u32[]{:S(2)}) async-start(bf16[32,4,512]{2,1,0:T(4,128)(2,1)} %broadcast_in_dim.4), calls=%async_computation.1 | async-start | bytes 262144 | tf_op jit(solution)/shard_map/all_to_all | solution.py:44
  66.7 106.3 %reduce-scatter.2.cloned.1.call-start = ((), (), s32[]{:S(2)}) async-start(), calls=%async_computation.6 | async-start | bytes 36864 | tf_op jit(solution)/shard_map/reduce_scatter | solution.py:166
  123.0 20.7 %copy-start.3 = (bf16[2048,128]{1,0:T(8,128)(2,1)S(1)}, bf16[2048,128]{1,0:T(8,128)(2,1)}, u32[]{:S(2)}) copy-start(bf16[2048,128]{1,0:T(8,128)(2,1)} %param.31) | copy-start | bytes 1572868
Sparse Core Ops, SparseCore 0:
  144.9 28.1 reduce-scatter.1
where the time goes:
time: 183 us; the launch traced here: 181 us
  blocking collectives  81.6 us (45%)
  waiting for transfers between devices  54.7 us (30%)
  starting transfers between devices  15.2 us (8%)
  between operations  14.4 us (8%)
  matrix products  6.81 us (4%)
  local copies, waits for them, and re-layouts  4.73 us (3%)
  other arithmetic  3.69 us (2%)
    all_gather x2, blocking collectives, gathered_rows(): gathered = lax.all_gather(stream, 'tp', axis=1, tiled=True)  29.7 us
    reduce_scatter x1, waiting for transfers between devices, shards(): lax.psum_scatter(down_rows.astype(jnp.bfloat16), 'tp', scatter_dimension=...  28.3 us
    all_to_all x1, blocking collectives, copy_for_each(): return lax.all_to_all(copies, axis, split_axis=0, concat_axis=0, tiled=True)  20.6 us
    all_to_all x1, blocking collectives, sent_and_summed(): lax.all_to_all(split_up(value, dim, length), axis, 0, 0, tiled=True)  20.2 us
    all_to_all x1, waiting for transfers between devices, sent_and_summed(): lax.all_to_all(split_up(value, dim, length), axis, 0, 0, tiled=True)  17.2 us
    all_to_all x1, blocking collectives, sent_and_summed_2(): lax.all_to_all(pieces, axis, split_axis=0, concat_axis=0, tiled=True)  11.1 us
    all_to_all x1, starting transfers between devices, sent_and_summed(): lax.all_to_all(split_up(value, dim, length), axis, 0, 0, tiled=True)  9.98 us
    all_to_all x1, waiting for transfers between devices, copy_for_each(): return lax.all_to_all(copies, axis, split_axis=0, concat_axis=0, tiled=True)  9.17 us
  transfers between devices with their start and end apart: 3, of which 3 were waited for; matrix products, arithmetic and copies ran while one was open for 0% of the time, Pallas kernels for 0%

commit v1 on v0

v1 whole, which is shorter than its diff:
```python
import functools

import jax
import jax.numpy as jnp
from jax import lax
from jax.experimental import pallas as pl
from jax.experimental.pallas import tpu as pltpu
from jax.sharding import PartitionSpec as P

MESH = pl.DeviceIdType.MESH
F32 = jnp.float32
BF16 = jnp.bfloat16
EPS = 1e-06
Y = 4
L = 128
HEADS_DEV = 4
ROWS = 4


def transposed(x):
    return jnp.transpose(x, (1, 0))


def silu(x):
    return x * jax.nn.sigmoid(x)


def softplus(x):
    return jnp.maximum(x, 0.0) + jnp.log1p(jnp.exp(-jnp.abs(x)))


def layer_kernel(
    Z,
    T,
    stream_ref,
    attn_gain_ref,
    mixer_gain_ref,
    head_gain_ref,
    beta_ref,
    decay_ref,
    decay_log_ref,
    decay_shift_ref,
    state_ref,
    wq_ref,
    wk_ref,
    wv_ref,
    wg_ref,
    wo_ref,
    wu_ref,
    wd_ref,
    out_ref,
    next_ref,
    state,
    state_out,
    w_in,
    wo,
    gains,
    etile,
    pad,
    sgath,
    w1,
    xz,
    s2,
    r2,
    rows_f,
    hall,
    a4,
    r4,
    mgath,
    wu,
    wd,
    sq,
    u6,
    r6,
    hall7,
    d8,
    r8,
    lsem,
    ssem,
    rsem,
):
    N = Z * Y
    PL = Y * T
    B = N * ROWS
    DT = L // T
    D = N * L
    kv = lax.axis_index("kv")
    tp = lax.axis_index("tp")
    z = lax.div(kv, Y)
    y = lax.rem(kv, Y)
    me_p = y * T + tp

    def plane_dev(p):
        return (z * Y + lax.div(p, T), lax.rem(p, T))

    def kv_dev(p):
        return (p, tp)

    def each_peer(n, me, act):
        def step(i, c):
            off = 1 + lax.rem(i + (n // 2 - 1), n - 1)
            act(lax.rem(me + off, n))
            return c

        lax.fori_loop(0, n - 1, step, 0)

    def put(src, dst, k, dev):
        pltpu.make_async_remote_copy(
            src_ref=src,
            dst_ref=dst,
            send_sem=ssem.at[k],
            recv_sem=rsem.at[k],
            device_id=dev,
            device_id_type=MESH,
        ).start()

    def got(ref, k):
        pltpu.make_async_copy(ref, ref, rsem.at[k]).wait()

    def sent(ref, k):
        pltpu.make_async_copy(ref, ref, ssem.at[k]).wait()

    barrier = pltpu.get_barrier_semaphore()

    def greet(dev):
        pl.semaphore_signal(barrier, inc=1, device_id=dev, device_id_type=MESH)

    each_peer(N, kv, lambda p: greet(kv_dev(p)))

    def greet_plane(p):
        @pl.when(lax.rem(p, T) != tp)
        def _():
            greet(plane_dev(p))

    each_peer(PL, me_p, greet_plane)

    loads = [
        pltpu.make_async_copy(w, w_in.at[m], lsem.at[m])
        for m, w in enumerate((wq_ref, wk_ref, wv_ref, wg_ref))
    ]
    load_out = pltpu.make_async_copy(wo_ref, wo, lsem.at[4])
    load_state = pltpu.make_async_copy(state_ref, state, lsem.at[5])
    for c in loads:
        c.start()
    load_out.start()
    load_state.start()

    gains[y] = jnp.broadcast_to(attn_gain_ref[...], (8, L))
    gains[y, 1:2, :] = mixer_gain_ref[...]
    pad[...] = jnp.zeros((L, L), F32)
    pad[:, 0:4] = beta_ref[...].astype(F32)
    pad[:, 4:8] = decay_ref[...].astype(F32)
    etile[y] = transposed(pad[...])[0:16].astype(BF16)
    pad[...] = jnp.zeros((L, L), F32)
    pad[0:B, 0:DT] = stream_ref[...].astype(F32)
    own_stream = transposed(pad[0:B, :])[0:DT]
    sgath[me_p] = own_stream.astype(BF16)

    pl.semaphore_wait(barrier, (N - 1) + (PL - 1) - (Y - 1))

    each_peer(PL, me_p, lambda p: put(sgath.at[me_p], sgath.at[me_p], 0, plane_dev(p)))
    for off in (2, 1, 3):
        yy = lax.rem(y + off, Y)
        put(gains.at[y], gains.at[y], 1, (z * Y + yy, tp))
        put(etile.at[y], etile.at[y], 2, (z * Y + yy, tp))
    for c in loads:
        c.wait()

    def head_cols(m, yy):
        return w_in.at[m, :, pl.ds(pl.multiple_of(yy * L, L), L)]

    def w1_cols(m):
        return w1.at[y, :, pl.ds(m * L, L)]

    own_w1 = [pltpu.make_async_copy(head_cols(m, y), w1_cols(m), lsem.at[6 + m]) for m in range(4)]
    for m in range(4):
        for off in (2, 1, 3):
            yy = lax.rem(y + off, Y)
            put(head_cols(m, yy), w1_cols(m), 3, (z * Y + yy, tp))
        own_w1[m].start()

    got(sgath.at[pl.ds(0, PL - 1)], 0)
    got(gains.at[pl.ds(0, Y - 1)], 1)
    got(etile.at[pl.ds(0, Y - 1)], 2)
    scaled = []
    x_part = jnp.zeros((16, B), F32)
    squares = jnp.zeros((1, B), F32)
    for j in range(Y):
        block = sgath[j * T : (j + 1) * T].astype(F32).reshape(L, B)
        squares = squares + jnp.sum(block * block, axis=0, keepdims=True)
        part = (transposed(block) * gains[j, 0:1, :]).astype(BF16)
        scaled.append(part)
        x_part = x_part + lax.dot_general(
            etile[j], part, (((1,), (1,)), ((), ())), preferred_element_type=F32
        )
    row16 = lax.broadcasted_iota(jnp.int32, (16, B), 0)
    xz[z] = jnp.where(row16 == 8, squares, x_part)
    for off in (4, 3, 5, 2, 6, 1, 7):
        if off < Z:
            zz = lax.rem(z + off, Z)
            put(xz.at[z], xz.at[z], 4, (zz * Y + y, tp))

    for c in own_w1:
        c.wait()
    got(w1.at[pl.ds(0, Y - 1)], 3)
    proj = jnp.zeros((B, 4 * L), F32)
    for j in range(Y):
        proj = proj + jnp.dot(scaled[j], w1[j], preferred_element_type=F32)
    low = lax.broadcasted_iota(jnp.int32, (B // 8, 8, L), 1) < 4

    def pair_tiles(a, b):
        return (
            jnp.where(low, a, pltpu.roll(b, 4, 1)),
            jnp.where(low, pltpu.roll(a, 4, 1), b),
        )

    pq, pk, pv, pg = [proj[:, m * L : (m + 1) * L].reshape(B // 8, 8, L) for m in range(4)]
    even_a, odd_a = pair_tiles(pq, pk)
    even_b, odd_b = pair_tiles(pv, pg)
    s2[:, 0] = jnp.concatenate([even_a, even_b], axis=1).astype(BF16)
    s2[:, 1] = jnp.concatenate([odd_a, odd_b], axis=1).astype(BF16)
    each_peer(
        N, kv, lambda p: put(s2.at[lax.div(p, 2), lax.rem(p, 2)], r2.at[kv], 5, kv_dev(p))
    )
    r2[kv] = s2[lax.div(kv, 2), lax.rem(kv, 2)]

    def up_cols(yy):
        return wu_ref.at[:, pl.ds(pl.multiple_of(yy * 4 * L, L), 4 * L)]

    own_up = pltpu.make_async_copy(up_cols(y), wu.at[y], lsem.at[10])
    own_up.start()
    for off in (2, 1, 3):
        yy = lax.rem(y + off, Y)
        put(up_cols(yy), wu.at[y], 6, (z * Y + yy, tp))

    got(xz.at[pl.ds(0, Z - 1)], 4)
    x_all = xz[0]
    for j in range(1, Z):
        x_all = x_all + xz[j]
    fac = lax.rsqrt(x_all[8:9] / D + EPS)
    xf = x_all * fac
    dlog = jnp.zeros((16, B), F32)
    dshift = jnp.zeros((16, B), F32)
    for h in range(HEADS_DEV):
        dlog = jnp.where(row16 == 4 + h, decay_log_ref[h], dlog)
        dshift = jnp.where(row16 == 4 + h, decay_shift_ref[h], dshift)
    scal = jnp.where(
        row16 < 4,
        jax.nn.sigmoid(xf),
        jnp.where(row16 < 8, jnp.exp(-jnp.exp(dlog) * softplus(xf + dshift)), fac),
    )
    lane_group = lax.div(lax.broadcasted_iota(jnp.int32, (16, B), 1), 4)
    mine = jnp.zeros((16, B), F32)
    for m in range(4):
        rolled = pltpu.roll(scal, lax.rem(B + m * ROWS - kv * ROWS, B), 1)
        mine = jnp.where(lane_group == m, rolled, mine)
    cols = transposed(jnp.concatenate([mine, jnp.zeros((L - 16, B), F32)], axis=0))[0:16]

    got(r2.at[pl.ds(0, N - 1)], 5)
    load_state.wait()
    row_id = lax.broadcasted_iota(jnp.int32, (16, 1), 0)
    acts = []
    for h in range(HEADS_DEV):
        total = r2[h].astype(F32)
        for j in range(1, Z):
            total = total + r2[j * Y + h].astype(F32)
        a = silu(total * cols[:, 8:9])
        inv = lax.rsqrt(jnp.sum(a * a, axis=1, keepdims=True) + EPS)
        norm = jnp.where(row_id < 4, inv * L ** (-0.5), jnp.where(row_id < 8, inv, 1.0))
        acts.append(a * norm)
        rows_f[1, 4 * h : 4 * h + 4, :] = a[12:16]
    flipped = transposed(jnp.concatenate(acts + [jnp.zeros((L - 64, L), F32)], axis=0))
    for h in range(HEADS_DEV):
        for r in range(ROWS):
            q_col = flipped[:, h * 16 + r : h * 16 + r + 1]
            k_col = flipped[:, h * 16 + 4 + r : h * 16 + 5 + r]
            kept = state[r, h] * cols[r : r + 1, 4 + h : 5 + h]
            recalled = jnp.sum(kept * k_col, axis=0, keepdims=True)
            corr = cols[r : r + 1, h : h + 1] * (acts[h][8 + r : 9 + r] - recalled)
            new = kept + k_col * corr
            state_out[r, h] = new
            rows_f[0, 4 * h + r : 4 * h + r + 1, :] = jnp.sum(new * q_col, axis=0, keepdims=True)
    readout = rows_f[0]
    readout = readout * lax.rsqrt(jnp.mean(readout * readout, axis=1, keepdims=True) + EPS)
    hall[kv] = (readout * head_gain_ref[...] * rows_f[1]).astype(BF16)

    each_peer(N, kv, lambda p: put(hall.at[kv], hall.at[kv], 7, kv_dev(p)))
    store_state = pltpu.make_async_copy(state_out, next_ref, lsem.at[11])
    store_state.start()

    def down_rows(yy):
        return wd_ref.at[pl.ds(pl.multiple_of(yy * 4 * L, L), 4 * L), :]

    own_down = pltpu.make_async_copy(down_rows(y), wd.at[y], lsem.at[12])
    own_down.start()
    for off in (2, 1, 3):
        yy = lax.rem(y + off, Y)
        put(down_rows(yy), wd.at[y], 8, (z * Y + yy, tp))

    load_out.wait()
    got(hall.at[pl.ds(0, N - 1)], 7)
    heads = hall[...].astype(F32).reshape(N // 2, 2, 2, 8, L)
    attn = jnp.zeros((B, L), F32)
    for c in range(2):
        h_even, h_odd = pair_tiles(heads[:, 0, c], heads[:, 1, c])
        for i, hh in ((2 * c, h_even), (2 * c + 1, h_odd)):
            attn = attn + jnp.dot(
                hh.reshape(B, L).astype(BF16),
                wo[i * L : (i + 1) * L, :],
                preferred_element_type=F32,
            )
    a4[...] = transposed(attn).reshape(T, DT, B).astype(BF16)
    each_peer(T, tp, lambda p: put(a4.at[p], r4.at[tp], 9, (kv, p)))
    r4[tp] = a4[tp]
    got(r4.at[pl.ds(0, T - 1)], 9)
    attn_mine = r4[0].astype(F32)
    for j in range(1, T):
        attn_mine = attn_mine + r4[j].astype(F32)
    middle = (own_stream + attn_mine).astype(BF16)

    mgath[me_p] = middle
    each_peer(PL, me_p, lambda p: put(mgath.at[me_p], mgath.at[me_p], 10, plane_dev(p)))
    own_up.wait()
    got(wu.at[pl.ds(0, Y - 1)], 6)
    got(mgath.at[pl.ds(0, PL - 1)], 10)
    up = jnp.zeros((B, 4 * L), F32)
    squares2 = jnp.zeros((1, B), F32)
    for j in range(Y):
        block = mgath[j * T : (j + 1) * T].astype(F32).reshape(L, B)
        squares2 = squares2 + jnp.sum(block * block, axis=0, keepdims=True)
        part = (transposed(block) * gains[j, 1:2, :]).astype(BF16)
        up = up + jnp.dot(part, wu[j], preferred_element_type=F32)
    u6[...] = up.astype(BF16).reshape(Z, 16, 4 * L)
    sq[z] = jnp.broadcast_to(squares2, (8, B))
    offs = [o for o in (4, 3, 5, 2, 6, 1, 7) if o < Z]
    for off in offs:
        zz = lax.rem(z + off, Z)
        put(u6.at[zz], r6.at[z], 11, (zz * Y + y, tp))
    for off in offs:
        zz = lax.rem(z + off, Z)
        put(sq.at[z], sq.at[z], 12, (zz * Y + y, tp))
    r6[z] = u6[z]
    got(r6.at[pl.ds(0, Z - 1)], 11)
    up_mine = r6[0].astype(F32)
    for j in range(1, Z):
        up_mine = up_mine + r6[j].astype(F32)
    hidden = jnp.square(jnp.maximum(up_mine, 0.0)).astype(BF16)
    hall7[z] = hidden
    for off in offs:
        zz = lax.rem(z + off, Z)
        put(hall7.at[z], hall7.at[z], 13, (zz * Y + y, tp))
    own_down.wait()
    got(wd.at[pl.ds(0, Y - 1)], 8)
    got(hall7.at[pl.ds(0, Z - 1)], 13)
    hid = hall7[...].reshape(B, 4 * L)
    for j in range(Y):
        part = jnp.dot(hid, wd[j], preferred_element_type=F32)
        d8[j * T : (j + 1) * T] = transposed(part).reshape(T, DT, B).astype(BF16)
    each_peer(PL, me_p, lambda p: put(d8.at[p], r8.at[me_p], 14, plane_dev(p)))
    r8[me_p] = d8[me_p]
    got(sq.at[pl.ds(0, Z - 1)], 12)
    total2 = sq[0, 0:1, :]
    for j in range(1, Z):
        total2 = total2 + sq[j, 0:1, :]
    factor2 = lax.rsqrt(total2 / D + EPS)
    got(r8.at[pl.ds(0, PL - 1)], 14)
    parts = [r8[j].astype(F32) for j in range(4)]
    for j in range(4, PL):
        parts[j % 4] = parts[j % 4] + r8[j].astype(F32)
    mixed = (parts[0] + parts[1]) + (parts[2] + parts[3])
    final = middle.astype(F32) + mixed * (factor2 * factor2)
    final = transposed(jnp.concatenate([final, jnp.zeros((L - DT, B), F32)], axis=0))
    out_ref[...] = final[:, 0:DT].astype(BF16)

    sent(sgath.at[pl.ds(0, PL - 1)], 0)
    sent(gains.at[pl.ds(0, Y - 1)], 1)
    sent(etile.at[pl.ds(0, Y - 1)], 2)
    sent(w1.at[pl.ds(0, Y - 1)], 3)
    sent(xz.at[pl.ds(0, Z - 1)], 4)
    sent(r2.at[pl.ds(0, N - 1)], 5)
    sent(wu.at[pl.ds(0, Y - 1)], 6)
    sent(hall.at[pl.ds(0, N - 1)], 7)
    sent(wd.at[pl.ds(0, Y - 1)], 8)
    sent(r4.at[pl.ds(0, T - 1)], 9)
    sent(mgath.at[pl.ds(0, PL - 1)], 10)
    sent(r6.at[pl.ds(0, Z - 1)], 11)
    sent(sq.at[pl.ds(0, Z - 1)], 12)
    sent(hall7.at[pl.ds(0, Z - 1)], 13)
    sent(r8.at[pl.ds(0, PL - 1)], 14)
    store_state.wait()


def shards(
    Z,
    T,
    stream,
    memory_state,
    attn_gain,
    query_weight,
    key_weight,
    value_weight,
    outgate_weight,
    beta_weight,
    decay_weight,
    decay_log,
    decay_shift,
    head_gain,
    output_weight,
    mixer_gain,
    up_weight,
    down_weight,
):
    N, PL, B, DT = Z * Y, Y * T, Z * Y * ROWS, L // T
    vmem = pl.BlockSpec(memory_space=pltpu.VMEM)
    smem = pl.BlockSpec(memory_space=pltpu.SMEM)
    hbm = pl.BlockSpec(memory_space=pl.ANY)
    layer_out, memory_next = pl.pallas_call(
        functools.partial(layer_kernel, Z, T),
        out_shape=(
            jax.ShapeDtypeStruct(stream.shape, BF16),
            jax.ShapeDtypeStruct(memory_state.shape, F32),
        ),
        in_specs=[vmem] * 6 + [smem] * 2 + [hbm] * 8,
        out_specs=(vmem, hbm),
        scratch_shapes=[
            pltpu.VMEM((ROWS, HEADS_DEV, L, L), F32),
            pltpu.VMEM((ROWS, HEADS_DEV, L, L), F32),
            pltpu.VMEM((4, L, 4 * L), BF16),
            pltpu.VMEM((4 * L, L), BF16),
            pltpu.VMEM((Y, 8, L), F32),
            pltpu.VMEM((Y, 16, L), BF16),
            pltpu.VMEM((L, L), F32),
            pltpu.VMEM((PL, DT, B), BF16),
            pltpu.VMEM((Y, L, 4 * L), BF16),
            pltpu.VMEM((Z, 16, B), F32),
            pltpu.VMEM((N // 2, 2, 16, L), BF16),
            pltpu.VMEM((N, 16, L), BF16),
            pltpu.VMEM((2, 16, L), F32),
            pltpu.VMEM((N, 16, L), BF16),
            pltpu.VMEM((T, DT, B), BF16),
            pltpu.VMEM((T, DT, B), BF16),
            pltpu.VMEM((PL, DT, B), BF16),
            pltpu.VMEM((Y, L, 4 * L), BF16),
            pltpu.VMEM((Y, 4 * L, L), BF16),
            pltpu.VMEM((Z, 8, B), F32),
            pltpu.VMEM((Z, 16, 4 * L), BF16),
            pltpu.VMEM((Z, 16, 4 * L), BF16),
            pltpu.VMEM((Z, 16, 4 * L), BF16),
            pltpu.VMEM((PL, DT, B), BF16),
            pltpu.VMEM((PL, DT, B), BF16),
            pltpu.SemaphoreType.DMA((16,)),
            pltpu.SemaphoreType.DMA((16,)),
            pltpu.SemaphoreType.DMA((16,)),
        ],
        compiler_params=pltpu.CompilerParams(collective_id=0, has_side_effects=True),
    )(
        stream,
        attn_gain.reshape(1, L),
        mixer_gain.reshape(1, L),
        head_gain.reshape(1, L),
        beta_weight,
        decay_weight,
        decay_log,
        decay_shift,
        memory_state,
        query_weight,
        key_weight,
        value_weight,
        outgate_weight,
        output_weight,
        up_weight,
        down_weight,
    )
    return layer_out, memory_next


def solution(mesh):
    in_specs = (
        P(None, ("kv", "tp")),
        P("kv", "tp", None, None),
        P("kv"),
        P("kv", "tp"),
        P("kv", "tp"),
        P("kv", "tp"),
        P("kv", "tp"),
        P("kv", "tp"),
        P("kv", "tp"),
        P("tp"),
        P("tp"),
        P(),
        P("tp", "kv"),
        P("kv"),
        P("kv", "tp"),
        P("tp", "kv"),
    )
    out_specs = (P(None, ("kv", "tp")), P("kv", "tp", None, None))
    body = functools.partial(shards, mesh.shape["kv"] // Y, mesh.shape["tp"])
    return jax.shard_map(body, mesh=mesh, in_specs=in_specs, out_specs=out_specs, check_vma=False)
```

time: 183 us -> 72.9 us (0.40)
  blocking collectives: 81.6 us -> 0 us
  Pallas kernels: 0 us -> 65.4 us
  waiting for transfers between devices: 54.7 us -> 0 us
  starting transfers between devices: 15.2 us -> 0 us
  between operations: 14.4 us -> 0.65 us
  matrix products: 6.81 us -> 0 us
  other arithmetic: 3.69 us -> 0 us
  local copies, waits for them, and re-layouts: 4.73 us -> 6.58 us
    pallas_call x0 -> x1, Pallas kernels: none -> 65.4 us  [shards(): pl.pallas_call(functools.partial(layer_kernel, Z, T), out_shape=(jax.Shap...]
    all_to_all x3 -> x0, blocking collectives: 51.9 us -> none  [the longest x1 20.6 us: copy_for_each(): return lax.all_to_all(copies, axis, split_axis=0, concat_axis=0, tiled=True)]
    all_gather x2 -> x0, blocking collectives: 29.7 us -> none  [gathered_rows(): gathered = lax.all_gather(stream, 'tp', axis=1, tiled=True)]
    reduce_scatter x1 -> x0, waiting for transfers between devices: 28.3 us -> none  [shards(): lax.psum_scatter(down_rows.astype(jnp.bfloat16), 'tp', scatter_dimension=...]
    all_to_all x2 -> x0, waiting for transfers between devices: 26.4 us -> none  [the longest x1 17.2 us: sent_and_summed(): lax.all_to_all(split_up(value, dim, length), axis, 0, 0, tiled=True)]
    all_to_all x2 -> x0, starting transfers between devices: 15.2 us -> none  [the longest x1 9.98 us: sent_and_summed(): lax.all_to_all(split_up(value, dim, length), axis, 0, 0, tiled=True)]
    dot_general x11 -> x0, matrix products: 6.81 us -> none  [the longest x6 4.74 us: product(): return jnp.dot(scaled, weight, preferred_element_type=jnp.float32)]
    unnamed x28 -> x10, local copies, waits for them, and re-layouts: 0.49 us -> 5.15 us
  transfers between devices with their start and end apart: 3 -> 0, of which waited for: 3 -> 0; matrix products, arithmetic and copies ran while one was open for 0% -> 0% of each run, Pallas kernels for 0% -> 0%
where the time goes in v1:
time: 72.9 us; the launch traced here: 72.6 us
  Pallas kernels  65.4 us (90%)
  local copies, waits for them, and re-layouts  6.58 us (9%)
    pallas_call x1, Pallas kernels, shards(): pl.pallas_call(functools.partial(layer_kernel, Z, T), out_shape=(jax.Shap...  65.4 us
    unnamed x10, local copies, waits for them, and re-layouts  5.15 us

profile of v1, /device:TPU:1, one launch (start us, length us, event | category | flops | bytes accessed | tf_op | source)
XLA Modules:
  0.0 72.6 jit_solution(1962074275577113901)
XLA Ops:
  0.6 0.0 copy-start
  0.6 0.7 copy-done
  1.3 0.0 copy-start.1
  1.3 0.7 copy.18.stream_ref
  2.0 0.0 copy-done.1
  2.0 0.0 copy-start.2
  2.0 0.7 %copy.19.beta_ref = bf16[128,4]{1,0:T(8,128)(2,1)} copy(bf16[128,4]{0,1:T(4,128)(2,1)S(1)} %copy-done.1) | data formatting | bytes 2048 | tf_op args[7]
  2.8 0.0 copy-done.2
  2.8 0.7 copy.20.decay_ref
  3.5 65.4 %shard_map.167 = (bf16[128,16]{1,0:T(8,128)(2,1)}, f32[4,4,128,128]{3,2,1,0:T(8,128)}) custom-call(bf16[128,16]{1,0:T(8,128)(2,1)} %copy.18.stream_ref, f32[1,128]{1,0:T(1,128)} %bitcast.3, f32[1,128]{1,0:T(1,128)} %bitcast.4, f32[1,128]{1,0:T(1,128)} %bitcast.5, bf16[128,4]{1,0:T(8,128)(2,1)} %copy.19.beta_ref, bf16[128,4]{1,0:T(8,128)(2,1)} %copy.20.decay_ref, ...), custom_call_target="tpu_custom_call" | custom-call | tf_op jit(solution)/shard_map/pallas_call | solution.py:417
  68.9 1.4 %copy.21 = bf16[128,16]{0,1:T(8,128)(2,1)} copy(bf16[128,16]{1,0:T(8,128)(2,1)} %get-tuple-element.2) | data formatting | bytes 8192 | tf_op jit(solution)/shard_map/pallas_call | solution.py:417
  70.4 2.3 %copy.23 = f32[4,4,128,128]{3,2,1,0:T(8,128)} copy(f32[4,4,128,128]{3,2,1,0:T(8,128)} %get-tuple-element.7) | data formatting | bytes 2097152
Async XLA Ops:
  0.6 0.7 copy-start
  1.3 0.7 copy-start.1
  2.0 0.7 %copy-start.2 = (bf16[128,4]{0,1:T(4,128)(2,1)S(1)}, bf16[128,4]{0,1:T(4,128)(2,1)}, u32[]{:S(2)}) copy-start(bf16[128,4]{0,1:T(4,128)(2,1)} %param.24) | copy-start | bytes 3076

commit v2 on v1

--- a/solution.py
+++ b/solution.py
@@ -32,14 +32,14 @@
 def layer_kernel(
     Z,
     T,
-    stream_ref,
-    attn_gain_ref,
-    mixer_gain_ref,
-    head_gain_ref,
-    beta_ref,
-    decay_ref,
-    decay_log_ref,
-    decay_shift_ref,
+    stream_hbm,
+    attn_gain_hbm,
+    mixer_gain_hbm,
+    head_gain_hbm,
+    beta_hbm,
+    decay_hbm,
+    decay_log_hbm,
+    decay_shift_hbm,
     state_ref,
     wq_ref,
     wk_ref,
@@ -50,13 +50,20 @@
     wd_ref,
     out_ref,
     next_ref,
+    stream_ref,
+    attn_gain_ref,
+    mixer_gain_ref,
+    head_gain_ref,
+    beta_ref,
+    decay_ref,
+    decay_log_ref,
+    decay_shift_ref,
     state,
     state_out,
     w_in,
     wo,
     gains,
     etile,
-    pad,
     sgath,
     w1,
     xz,
@@ -75,6 +82,7 @@
     hall7,
     d8,
     r8,
+    layer,
     lsem,
     ssem,
     rsem,
@@ -115,7 +123,8 @@
         ).start()
 
     def got(ref, k):
-        pltpu.make_async_copy(ref, ref, rsem.at[k]).wait()
+        with jax.named_scope(f"got{k}"):
+            pltpu.make_async_copy(ref, ref, rsem.at[k]).wait()
 
     def sent(ref, k):
         pltpu.make_async_copy(ref, ref, ssem.at[k]).wait()
@@ -138,25 +147,47 @@
         pltpu.make_async_copy(w, w_in.at[m], lsem.at[m])
         for m, w in enumerate((wq_ref, wk_ref, wv_ref, wg_ref))
     ]
+    small = [
+        pltpu.make_async_copy(a, b, lsem.at[16 + i])
+        for i, (a, b) in enumerate((
+            (stream_hbm, stream_ref),
+            (attn_gain_hbm, attn_gain_ref),
+            (mixer_gain_hbm, mixer_gain_ref),
+            (beta_hbm, beta_ref),
+            (decay_hbm, decay_ref),
+        ))
+    ]
+    late = [
+        pltpu.make_async_copy(a, b, lsem.at[21 + i])
+        for i, (a, b) in enumerate((
+            (head_gain_hbm, head_gain_ref),
+            (decay_log_hbm, decay_log_ref),
+            (decay_shift_hbm, decay_shift_ref),
+        ))
+    ]
+    for c in small:
+        c.start()
     load_out = pltpu.make_async_copy(wo_ref, wo, lsem.at[4])
     load_state = pltpu.make_async_copy(state_ref, state, lsem.at[5])
     for c in loads:
         c.start()
     load_out.start()
     load_state.start()
-
+    for c in late:
+        c.start()
+
+    for c in small:
+        c.wait()
     gains[y] = jnp.broadcast_to(attn_gain_ref[...], (8, L))
     gains[y, 1:2, :] = mixer_gain_ref[...]
-    pad[...] = jnp.zeros((L, L), F32)
-    pad[:, 0:4] = beta_ref[...].astype(F32)
-    pad[:, 4:8] = decay_ref[...].astype(F32)
-    etile[y] = transposed(pad[...])[0:16].astype(BF16)
-    pad[...] = jnp.zeros((L, L), F32)
-    pad[0:B, 0:DT] = stream_ref[...].astype(F32)
-    own_stream = transposed(pad[0:B, :])[0:DT]
-    sgath[me_p] = own_stream.astype(BF16)
-
-    pl.semaphore_wait(barrier, (N - 1) + (PL - 1) - (Y - 1))
+    etile[y] = jnp.concatenate(
+        [beta_ref[...].astype(F32), decay_ref[...].astype(F32), jnp.zeros((8, L), F32)], axis=0
+    ).astype(BF16)
+    own_stream = stream_ref[...].astype(F32)
+    sgath[me_p] = stream_ref[...]
+
+    with jax.named_scope("greeted"):
+        pl.semaphore_wait(barrier, (N - 1) + (PL - 1) - (Y - 1))
 
     each_peer(PL, me_p, lambda p: put(sgath.at[me_p], sgath.at[me_p], 0, plane_dev(p)))
     for off in (2, 1, 3):
@@ -233,6 +264,8 @@
         yy = lax.rem(y + off, Y)
         put(up_cols(yy), wu.at[y], 6, (z * Y + yy, tp))
 
+    for c in late:
+        c.wait()
     got(xz.at[pl.ds(0, Z - 1)], 4)
     x_all = xz[0]
     for j in range(1, Z):
@@ -369,8 +402,9 @@
         parts[j % 4] = parts[j % 4] + r8[j].astype(F32)
     mixed = (parts[0] + parts[1]) + (parts[2] + parts[3])
     final = middle.astype(F32) + mixed * (factor2 * factor2)
-    final = transposed(jnp.concatenate([final, jnp.zeros((L - DT, B), F32)], axis=0))
-    out_ref[...] = final[:, 0:DT].astype(BF16)
+    layer[...] = final.astype(BF16)
+    store_layer = pltpu.make_async_copy(layer, out_ref, lsem.at[15])
+    store_layer.start()
 
     sent(sgath.at[pl.ds(0, PL - 1)], 0)
     sent(gains.at[pl.ds(0, Y - 1)], 1)
@@ -388,6 +422,18 @@
     sent(hall7.at[pl.ds(0, Z - 1)], 13)
     sent(r8.at[pl.ds(0, PL - 1)], 14)
     store_state.wait()
+    store_layer.wait()
+
+
+def hand_over(layer_in, state_in, layer_ref, state_ref, sems):
+    copies = [
+        pltpu.make_async_copy(state_in, state_ref, sems.at[0]),
+        pltpu.make_async_copy(layer_in, layer_ref, sems.at[1]),
+    ]
+    for c in copies:
+        c.start()
+    for c in copies:
+        c.wait()
 
 
 def shards(
@@ -411,25 +457,31 @@
     down_weight,
 ):
     N, PL, B, DT = Z * Y, Y * T, Z * Y * ROWS, L // T
-    vmem = pl.BlockSpec(memory_space=pltpu.VMEM)
-    smem = pl.BlockSpec(memory_space=pltpu.SMEM)
-    hbm = pl.BlockSpec(memory_space=pl.ANY)
+    hbm = pl.BlockSpec(memory_space=pltpu.HBM)
+    anywhere = pl.BlockSpec(memory_space=pl.ANY)
     layer_out, memory_next = pl.pallas_call(
         functools.partial(layer_kernel, Z, T),
         out_shape=(
-            jax.ShapeDtypeStruct(stream.shape, BF16),
-            jax.ShapeDtypeStruct(memory_state.shape, F32),
+            pltpu.VMEM((DT, B), BF16),
+            pltpu.VMEM(memory_state.shape, F32),
         ),
-        in_specs=[vmem] * 6 + [smem] * 2 + [hbm] * 8,
-        out_specs=(vmem, hbm),
+        in_specs=[hbm] * 16,
+        out_specs=(anywhere, anywhere),
         scratch_shapes=[
+            pltpu.VMEM((DT, B), BF16),
+            pltpu.VMEM((1, L), F32),
+            pltpu.VMEM((1, L), F32),
+            pltpu.VMEM((1, L), F32),
+            pltpu.VMEM((HEADS_DEV, L), BF16),
+            pltpu.VMEM((HEADS_DEV, L), BF16),
+            pltpu.SMEM((HEADS_DEV,), F32),
+            pltpu.SMEM((HEADS_DEV,), F32),
             pltpu.VMEM((ROWS, HEADS_DEV, L, L), F32),
             pltpu.VMEM((ROWS, HEADS_DEV, L, L), F32),
             pltpu.VMEM((4, L, 4 * L), BF16),
             pltpu.VMEM((4 * L, L), BF16),
             pltpu.VMEM((Y, 8, L), F32),
             pltpu.VMEM((Y, 16, L), BF16),
-            pltpu.VMEM((L, L), F32),
             pltpu.VMEM((PL, DT, B), BF16),
             pltpu.VMEM((Y, L, 4 * L), BF16),
             pltpu.VMEM((Z, 16, B), F32),
@@ -448,18 +500,23 @@
             pltpu.VMEM((Z, 16, 4 * L), BF16),
             pltpu.VMEM((PL, DT, B), BF16),
             pltpu.VMEM((PL, DT, B), BF16),
-            pltpu.SemaphoreType.DMA((16,)),
+            pltpu.VMEM((DT, B), BF16),
+            pltpu.SemaphoreType.DMA((24,)),
             pltpu.SemaphoreType.DMA((16,)),
             pltpu.SemaphoreType.DMA((16,)),
         ],
-        compiler_params=pltpu.CompilerParams(collective_id=0, has_side_effects=True),
+        compiler_params=pltpu.CompilerParams(
+            collective_id=0,
+            has_side_effects=True,
+            vmem_limit_bytes=67043328 - memory_state.size * 4 - 8192,
+        ),
     )(
-        stream,
+        stream.T,
         attn_gain.reshape(1, L),
         mixer_gain.reshape(1, L),
         head_gain.reshape(1, L),
-        beta_weight,
-        decay_weight,
+        beta_weight.T,
+        decay_weight.T,
         decay_log,
         decay_shift,
         memory_state,
@@ -471,7 +528,18 @@
         up_weight,
         down_weight,
     )
-    return layer_out, memory_next
+    layer_out, memory_next = pl.pallas_call(
+        hand_over,
+        out_shape=(
+            jax.ShapeDtypeStruct((DT, B), BF16),
+            jax.ShapeDtypeStruct(memory_state.shape, F32),
+        ),
+        in_specs=[anywhere] * 2,
+        out_specs=(hbm, hbm),
+        scratch_shapes=[pltpu.SemaphoreType.DMA((2,))],
+        compiler_params=pltpu.CompilerParams(vmem_limit_bytes=2**20),
+    )(layer_out, memory_next)
+    return layer_out.T, memory_next
 
 
 def solution(mesh):

time: 72.9 us -> 65.7 us (0.901)
  local copies, waits for them, and re-layouts: 6.58 us -> 0 us
    unnamed x10 -> x0, local copies, waits for them, and re-layouts: 5.15 us -> none
    pallas_call x1 -> x0, local copies, waits for them, and re-layouts: 1.42 us -> none  [shards(): pl.pallas_call(functools.partial(layer_kernel, Z, T), out_shape=(jax.Shap...]
    pallas_call x1 -> x2, Pallas kernels: 65.4 us -> 64.9 us  [the longest x1 63.9 us: shards(): pl.pallas_call(functools.partial(layer_kernel, Z, T), out_shape=(pltpu.VM...]
where the time goes in v2:
time: 65.7 us; the launch traced here: 65.6 us
  Pallas kernels  64.9 us (99%)
    pallas_call x1, Pallas kernels, shards(): pl.pallas_call(functools.partial(layer_kernel, Z, T), out_shape=(pltpu.VM...  63.9 us

profile of v2, /device:TPU:1, one launch (start us, length us, event | category | flops | bytes accessed | tf_op | source)
XLA Modules:
  0.0 65.6 jit_solution(13495225750994055502)
XLA Ops:
  0.6 63.9 %shard_map.167 = (bf16[16,128]{1,0:T(8,128)(2,1)S(1)}, f32[4,4,128,128]{3,2,1,0:T(8,128)S(1)}) custom-call(bf16[16,128]{1,0:T(8,128)(2,1)} %bitcast.7, f32[1,128]{1,0:T(1,128)} %bitcast.10, f32[1,128]{1,0:T(1,128)} %bitcast.11, f32[1,128]{1,0:T(1,128)} %bitcast.12, bf16[4,128]{1,0:T(4,128)(2,1)} %bitcast.8, bf16[4,128]{1,0:T(4,128)(2,1)} %bitcast.9, ...), custom_call_target="tpu_custom_call" | custom-call | tf_op jit(solution)/shard_map/pallas_call | solution.py:462
  64.6 1.0 %shard_map.168 = (bf16[16,128]{1,0:T(8,128)(2,1)}, f32[4,4,128,128]{3,2,1,0:T(8,128)}) custom-call(bf16[16,128]{1,0:T(8,128)(2,1)S(1)} %get-tuple-element.6.layer_in, f32[4,4,128,128]{3,2,1,0:T(8,128)S(1)} %get-tuple-element.7.state_in), custom_call_target="tpu_custom_call" | custom-call | tf_op jit(solution)/shard_map/pallas_call | solution.py:531

commit v3 on v2

--- a/solution.py
+++ b/solution.py
@@ -59,7 +59,6 @@
     decay_log_ref,
     decay_shift_ref,
     state,
-    state_out,
     w_in,
     wo,
     gains,
@@ -82,7 +81,10 @@
     hall7,
     d8,
     r8,
-    layer,
+    wot,
+    wut,
+    wdt,
+    gcol,
     lsem,
     ssem,
     rsem,
@@ -128,20 +130,6 @@
 
     def sent(ref, k):
         pltpu.make_async_copy(ref, ref, ssem.at[k]).wait()
-
-    barrier = pltpu.get_barrier_semaphore()
-
-    def greet(dev):
-        pl.semaphore_signal(barrier, inc=1, device_id=dev, device_id_type=MESH)
-
-    each_peer(N, kv, lambda p: greet(kv_dev(p)))
-
-    def greet_plane(p):
-        @pl.when(lax.rem(p, T) != tp)
-        def _():
-            greet(plane_dev(p))
-
-    each_peer(PL, me_p, greet_plane)
 
     loads = [
         pltpu.make_async_copy(w, w_in.at[m], lsem.at[m])
@@ -176,6 +164,17 @@
     for c in late:
         c.start()
 
+    barrier = pltpu.get_barrier_semaphore()
+
+    def greet(dev):
+        pl.semaphore_signal(barrier, inc=1, device_id=dev, device_id_type=MESH)
+
+    with jax.named_scope("greet"):
+        for off in (4, 3, 5, 2, 6, 1, 7):
+            if off < Z:
+                greet((lax.rem(z + off, Z) * Y + y, tp))
+        each_peer(PL, me_p, lambda p: greet(plane_dev(p)))
+
     for c in small:
         c.wait()
     gains[y] = jnp.broadcast_to(attn_gain_ref[...], (8, L))
@@ -187,7 +186,7 @@
     sgath[me_p] = stream_ref[...]
 
     with jax.named_scope("greeted"):
-        pl.semaphore_wait(barrier, (N - 1) + (PL - 1) - (Y - 1))
+        pl.semaphore_wait(barrier, (Z - 1) + (PL - 1))
 
     each_peer(PL, me_p, lambda p: put(sgath.at[me_p], sgath.at[me_p], 0, plane_dev(p)))
     for off in (2, 1, 3):
@@ -311,15 +310,13 @@
             recalled = jnp.sum(kept * k_col, axis=0, keepdims=True)
             corr = cols[r : r + 1, h : h + 1] * (acts[h][8 + r : 9 + r] - recalled)
             new = kept + k_col * corr
-            state_out[r, h] = new
+            next_ref[r, h] = new
             rows_f[0, 4 * h + r : 4 * h + r + 1, :] = jnp.sum(new * q_col, axis=0, keepdims=True)
     readout = rows_f[0]
     readout = readout * lax.rsqrt(jnp.mean(readout * readout, axis=1, keepdims=True) + EPS)
     hall[kv] = (readout * head_gain_ref[...] * rows_f[1]).astype(BF16)
 
     each_peer(N, kv, lambda p: put(hall.at[kv], hall.at[kv], 7, kv_dev(p)))
-    store_state = pltpu.make_async_copy(state_out, next_ref, lsem.at[11])
-    store_state.start()
 
     def down_rows(yy):
         return wd_ref.at[pl.ds(pl.multiple_of(yy * 4 * L, L), 4 * L), :]
@@ -331,18 +328,29 @@
         put(down_rows(yy), wd.at[y], 8, (z * Y + yy, tp))
 
     load_out.wait()
+    for i in range(HEADS_DEV):
+        wot[:, i * L : (i + 1) * L] = transposed(wo[i * L : (i + 1) * L, :].astype(F32)).astype(BF16)
+    own_up.wait()
+    got(wu.at[pl.ds(0, Y - 1)], 6)
+    for j in range(Y):
+        for i in range(4):
+            wut[i * L : (i + 1) * L, j * L : (j + 1) * L] = transposed(
+                wu[j, :, i * L : (i + 1) * L].astype(F32)
+            ).astype(BF16)
+        gcol[j] = transposed(jnp.broadcast_to(gains[j, 1:2, :], (B, L)))
     got(hall.at[pl.ds(0, N - 1)], 7)
     heads = hall[...].astype(F32).reshape(N // 2, 2, 2, 8, L)
-    attn = jnp.zeros((B, L), F32)
+    attn = jnp.zeros((L, B), F32)
     for c in range(2):
         h_even, h_odd = pair_tiles(heads[:, 0, c], heads[:, 1, c])
         for i, hh in ((2 * c, h_even), (2 * c + 1, h_odd)):
-            attn = attn + jnp.dot(
+            attn = attn + lax.dot_general(
+                wot[:, i * L : (i + 1) * L],
                 hh.reshape(B, L).astype(BF16),
-                wo[i * L : (i + 1) * L, :],
+                (((1,), (1,)), ((), ())),
                 preferred_element_type=F32,
             )
-    a4[...] = transposed(attn).reshape(T, DT, B).astype(BF16)
+    a4[...] = attn.reshape(T, DT, B).astype(BF16)
     each_peer(T, tp, lambda p: put(a4.at[p], r4.at[tp], 9, (kv, p)))
     r4[tp] = a4[tp]
     got(r4.at[pl.ds(0, T - 1)], 9)
@@ -353,26 +361,28 @@
 
     mgath[me_p] = middle
     each_peer(PL, me_p, lambda p: put(mgath.at[me_p], mgath.at[me_p], 10, plane_dev(p)))
-    own_up.wait()
-    got(wu.at[pl.ds(0, Y - 1)], 6)
     got(mgath.at[pl.ds(0, PL - 1)], 10)
-    up = jnp.zeros((B, 4 * L), F32)
+    up = jnp.zeros((4 * L, B), F32)
     squares2 = jnp.zeros((1, B), F32)
     for j in range(Y):
         block = mgath[j * T : (j + 1) * T].astype(F32).reshape(L, B)
         squares2 = squares2 + jnp.sum(block * block, axis=0, keepdims=True)
-        part = (transposed(block) * gains[j, 1:2, :]).astype(BF16)
-        up = up + jnp.dot(part, wu[j], preferred_element_type=F32)
-    u6[...] = up.astype(BF16).reshape(Z, 16, 4 * L)
+        part = (block * gcol[j]).astype(BF16)
+        up = up + jnp.dot(wut[:, j * L : (j + 1) * L], part, preferred_element_type=F32)
+    u6[...] = up.astype(BF16).reshape(Z, 4 * L // Z, B)
     sq[z] = jnp.broadcast_to(squares2, (8, B))
     offs = [o for o in (4, 3, 5, 2, 6, 1, 7) if o < Z]
     for off in offs:
         zz = lax.rem(z + off, Z)
         put(u6.at[zz], r6.at[z], 11, (zz * Y + y, tp))
-    for off in offs:
-        zz = lax.rem(z + off, Z)
-        put(sq.at[z], sq.at[z], 12, (zz * Y + y, tp))
     r6[z] = u6[z]
+    own_down.wait()
+    got(wd.at[pl.ds(0, Y - 1)], 8)
+    for j in range(Y):
+        for i in range(4):
+            wdt[j * L : (j + 1) * L, i * L : (i + 1) * L] = transposed(
+                wd[j, i * L : (i + 1) * L, :].astype(F32)
+            ).astype(BF16)
     got(r6.at[pl.ds(0, Z - 1)], 11)
     up_mine = r6[0].astype(F32)
     for j in range(1, Z):
@@ -382,13 +392,12 @@
     for off in offs:
         zz = lax.rem(z + off, Z)
         put(hall7.at[z], hall7.at[z], 13, (zz * Y + y, tp))
-    own_down.wait()
-    got(wd.at[pl.ds(0, Y - 1)], 8)
+    for off in offs:
+        zz = lax.rem(z + off, Z)
+        put(sq.at[z], sq.at[z], 12, (zz * Y + y, tp))
     got(hall7.at[pl.ds(0, Z - 1)], 13)
-    hid = hall7[...].reshape(B, 4 * L)
-    for j in range(Y):
-        part = jnp.dot(hid, wd[j], preferred_element_type=F32)
-        d8[j * T : (j + 1) * T] = transposed(part).reshape(T, DT, B).astype(BF16)
+    down = jnp.dot(wdt[...], hall7[...].reshape(4 * L, B), preferred_element_type=F32)
+    d8[...] = down.reshape(PL, DT, B).astype(BF16)
     each_peer(PL, me_p, lambda p: put(d8.at[p], r8.at[me_p], 14, plane_dev(p)))
     r8[me_p] = d8[me_p]
     got(sq.at[pl.ds(0, Z - 1)], 12)
@@ -402,9 +411,7 @@
         parts[j % 4] = parts[j % 4] + r8[j].astype(F32)
     mixed = (parts[0] + parts[1]) + (parts[2] + parts[3])
     final = middle.astype(F32) + mixed * (factor2 * factor2)
-    layer[...] = final.astype(BF16)
-    store_layer = pltpu.make_async_copy(layer, out_ref, lsem.at[15])
-    store_layer.start()
+    out_ref[...] = final.astype(BF16)
 
     sent(sgath.at[pl.ds(0, PL - 1)], 0)
     sent(gains.at[pl.ds(0, Y - 1)], 1)
@@ -421,15 +428,12 @@
     sent(sq.at[pl.ds(0, Z - 1)], 12)
     sent(hall7.at[pl.ds(0, Z - 1)], 13)
     sent(r8.at[pl.ds(0, PL - 1)], 14)
-    store_state.wait()
-    store_layer.wait()
 
 
 def hand_over(layer_in, state_in, layer_ref, state_ref, sems):
-    copies = [
-        pltpu.make_async_copy(state_in, state_ref, sems.at[0]),
-        pltpu.make_async_copy(layer_in, layer_ref, sems.at[1]),
-    ]
+    copies = [pltpu.make_async_copy(layer_in, layer_ref, sems.at[4])]
+    for r in range(ROWS):
+        copies.append(pltpu.make_async_copy(state_in.at[r], state_ref.at[r], sems.at[r]))
     for c in copies:
         c.start()
     for c in copies:
@@ -459,6 +463,7 @@
     N, PL, B, DT = Z * Y, Y * T, Z * Y * ROWS, L // T
     hbm = pl.BlockSpec(memory_space=pltpu.HBM)
     anywhere = pl.BlockSpec(memory_space=pl.ANY)
+    vmem = pl.BlockSpec(memory_space=pltpu.VMEM)
     layer_out, memory_next = pl.pallas_call(
         functools.partial(layer_kernel, Z, T),
         out_shape=(
@@ -466,7 +471,7 @@
             pltpu.VMEM(memory_state.shape, F32),
         ),
         in_specs=[hbm] * 16,
-        out_specs=(anywhere, anywhere),
+        out_specs=(vmem, vmem),
         scratch_shapes=[
             pltpu.VMEM((DT, B), BF16),
             pltpu.VMEM((1, L), F32),
@@ -476,7 +481,6 @@
             pltpu.VMEM((HEADS_DEV, L), BF16),
             pltpu.SMEM((HEADS_DEV,), F32),
             pltpu.SMEM((HEADS_DEV,), F32),
-            pltpu.VMEM((ROWS, HEADS_DEV, L, L), F32),
             pltpu.VMEM((ROWS, HEADS_DEV, L, L), F32),
             pltpu.VMEM((4, L, 4 * L), BF16),
             pltpu.VMEM((4 * L, L), BF16),
@@ -495,12 +499,15 @@
             pltpu.VMEM((Y, L, 4 * L), BF16),
             pltpu.VMEM((Y, 4 * L, L), BF16),
             pltpu.VMEM((Z, 8, B), F32),
-            pltpu.VMEM((Z, 16, 4 * L), BF16),
-            pltpu.VMEM((Z, 16, 4 * L), BF16),
-            pltpu.VMEM((Z, 16, 4 * L), BF16),
+            pltpu.VMEM((Z, 4 * L // Z, B), BF16),
+            pltpu.VMEM((Z, 4 * L // Z, B), BF16),
+            pltpu.VMEM((Z, 4 * L // Z, B), BF16),
             pltpu.VMEM((PL, DT, B), BF16),
             pltpu.VMEM((PL, DT, B), BF16),
-            pltpu.VMEM((DT, B), BF16),
+            pltpu.VMEM((L, 4 * L), BF16),
+            pltpu.VMEM((4 * L, 4 * L), BF16),
+            pltpu.VMEM((4 * L, 4 * L), BF16),
+            pltpu.VMEM((Y, L, B), F32),
             pltpu.SemaphoreType.DMA((24,)),
             pltpu.SemaphoreType.DMA((16,)),
             pltpu.SemaphoreType.DMA((16,)),
@@ -536,7 +543,7 @@
         ),
         in_specs=[anywhere] * 2,
         out_specs=(hbm, hbm),
-        scratch_shapes=[pltpu.SemaphoreType.DMA((2,))],
+        scratch_shapes=[pltpu.SemaphoreType.DMA((5,))],
         compiler_params=pltpu.CompilerParams(vmem_limit_bytes=2**20),
     )(layer_out, memory_next)
     return layer_out.T, memory_next

time: 65.7 us -> 65 us (0.989)
  Pallas kernels: 64.9 us -> 64.2 us
    pallas_call x1, Pallas kernels: 63.9 us -> 63.2 us  [shards(): pl.pallas_call(functools.partial(layer_kernel, Z, T), out_shape=(pltpu.VM...]
where the time goes in v3:
time: 65 us; the launch traced here: 64.9 us
  Pallas kernels  64.2 us (99%)
    pallas_call x1, Pallas kernels, shards(): pl.pallas_call(functools.partial(layer_kernel, Z, T), out_shape=(pltpu.VM...  63.2 us

profile of v3, /device:TPU:1, one launch (start us, length us, event | category | flops | bytes accessed | tf_op | source)
XLA Modules:
  0.0 64.9 jit_solution(1684091304294412493)
XLA Ops:
  0.6 63.2 %shard_map.167 = (bf16[16,128]{1,0:T(8,128)(2,1)S(1)}, f32[4,4,128,128]{3,2,1,0:T(8,128)S(1)}) custom-call(bf16[16,128]{1,0:T(8,128)(2,1)} %bitcast.7, f32[1,128]{1,0:T(1,128)} %bitcast.10, f32[1,128]{1,0:T(1,128)} %bitcast.11, f32[1,128]{1,0:T(1,128)} %bitcast.12, bf16[4,128]{1,0:T(4,128)(2,1)} %bitcast.8, bf16[4,128]{1,0:T(4,128)(2,1)} %bitcast.9, ...), custom_call_target="tpu_custom_call" | custom-call | tf_op jit(solution)/shard_map/pallas_call | solution.py:467
  63.9 1.0 %shard_map.168 = (bf16[16,128]{1,0:T(8,128)(2,1)}, f32[4,4,128,128]{3,2,1,0:T(8,128)}) custom-call(bf16[16,128]{1,0:T(8,128)(2,1)S(1)} %get-tuple-element.6.layer_in, f32[4,4,128,128]{3,2,1,0:T(8,128)S(1)} %get-tuple-element.7.state_in), custom_call_target="tpu_custom_call" | custom-call | tf_op jit(solution)/shard_map/pallas_call | solution.py:538

commit v4 on v3

--- a/solution.py
+++ b/solution.py
@@ -23,6 +23,12 @@
 
 def silu(x):
     return x * jax.nn.sigmoid(x)
+
+
+def added(parts):
+    while len(parts) > 1:
+        parts = [a + b for a, b in zip(parts[::2], parts[1::2])] + parts[len(parts) // 2 * 2 :]
+    return parts[0]
 
 
 def softplus(x):
@@ -61,7 +67,7 @@
     state,
     w_in,
     wo,
-    gains,
+    gpos,
     etile,
     sgath,
     w1,
@@ -99,6 +105,15 @@
     z = lax.div(kv, Y)
     y = lax.rem(kv, Y)
     me_p = y * T + tp
+    pz, py = lax.rem(z, 2), lax.rem(y, 2)
+    za, zb = z + 1 - 2 * pz, lax.rem(z - 1 + 2 * pz + Z, Z)
+    ya, yb = y + 1 - 2 * py, lax.rem(y - 1 + 2 * py + Y, Y)
+    spots = [kv, za * Y + y, z * Y + ya, za * Y + ya, zb * Y + y, z * Y + yb, zb * Y + yb]
+    spot_far = z * Y + lax.rem(y + 2, Y)
+    head_a = pz * 2 + py
+    heads_a = [head_a, (1 - pz) * 2 + py, pz * 2 + 1 - py, (1 - pz) * 2 + 1 - py]
+    groups = ((0, (0, 1, 2, 3)), (1, (0, 4, 5, 6)))
+    tps = [lax.rem(tp + i, T) for i in range(T)]
 
     def plane_dev(p):
         return (z * Y + lax.div(p, T), lax.rem(p, T))
@@ -170,72 +185,104 @@
         pl.semaphore_signal(barrier, inc=1, device_id=dev, device_id_type=MESH)
 
     with jax.named_scope("greet"):
-        for off in (4, 3, 5, 2, 6, 1, 7):
-            if off < Z:
-                greet((lax.rem(z + off, Z) * Y + y, tp))
-        each_peer(PL, me_p, lambda p: greet(plane_dev(p)))
+        for dst in reversed(spots[1:]):
+            for t in tps:
+                greet((dst, t))
+        for off in (4, 3, 5, 2, 6):
+            greet((lax.rem(z + off, Z) * Y + y, tp))
+        greet((spot_far, tp))
+        for t in tps[1:]:
+            greet((kv, t))
 
     for c in small:
         c.wait()
-    gains[y] = jnp.broadcast_to(attn_gain_ref[...], (8, L))
-    gains[y, 1:2, :] = mixer_gain_ref[...]
-    etile[y] = jnp.concatenate(
+    gpos[0] = jnp.broadcast_to(attn_gain_ref[...], (8, L))
+    gpos[0, 1:2, :] = mixer_gain_ref[...]
+    etile[0] = jnp.concatenate(
         [beta_ref[...].astype(F32), decay_ref[...].astype(F32), jnp.zeros((8, L), F32)], axis=0
     ).astype(BF16)
     own_stream = stream_ref[...].astype(F32)
-    sgath[me_p] = stream_ref[...]
+    sgath[0, tp] = stream_ref[...]
 
     with jax.named_scope("greeted"):
-        pl.semaphore_wait(barrier, (Z - 1) + (PL - 1))
-
-    each_peer(PL, me_p, lambda p: put(sgath.at[me_p], sgath.at[me_p], 0, plane_dev(p)))
-    for off in (2, 1, 3):
-        yy = lax.rem(y + off, Y)
-        put(gains.at[y], gains.at[y], 1, (z * Y + yy, tp))
-        put(etile.at[y], etile.at[y], 2, (z * Y + yy, tp))
+        pl.semaphore_wait(barrier, 7 * T - 1 + (Z - 3) + 1)
+
+    for k in (3, 6, 1, 2, 4, 5):
+        for t in tps:
+            put(sgath.at[0, tp], sgath.at[k, tp], 16 + k, (spots[k], t))
+    for t in tps[1:]:
+        put(sgath.at[0, tp], sgath.at[0, tp], 16, (kv, t))
+    for k in range(1, 7):
+        put(gpos.at[0], gpos.at[k], 1, (spots[k], tp))
+        if k < 4:
+            put(etile.at[0], etile.at[k], 2, (spots[k], tp))
+    put(gpos.at[0], gpos.at[7], 1, (spot_far, tp))
     for c in loads:
         c.wait()
 
-    def head_cols(m, yy):
-        return w_in.at[m, :, pl.ds(pl.multiple_of(yy * L, L), L)]
-
-    def w1_cols(m):
-        return w1.at[y, :, pl.ds(m * L, L)]
-
-    own_w1 = [pltpu.make_async_copy(head_cols(m, y), w1_cols(m), lsem.at[6 + m]) for m in range(4)]
-    for m in range(4):
-        for off in (2, 1, 3):
-            yy = lax.rem(y + off, Y)
-            put(head_cols(m, yy), w1_cols(m), 3, (z * Y + yy, tp))
-        own_w1[m].start()
-
-    got(sgath.at[pl.ds(0, PL - 1)], 0)
-    got(gains.at[pl.ds(0, Y - 1)], 1)
-    got(etile.at[pl.ds(0, Y - 1)], 2)
-    scaled = []
+    def head_cols(m, h):
+        return w_in.at[m, :, pl.ds(pl.multiple_of(h * L, L), L)]
+
+    own_w1 = []
+    for g, members in groups:
+        for slot in (3, 1, 2):
+            h = heads_a[slot]
+            h = h if g == 0 else 3 - h
+            for i in range(2):
+                put(
+                    head_cols(2 * g + i, h),
+                    w1.at[g, slot, :, pl.ds(i * L, L)],
+                    3,
+                    (spots[members[slot]], tp),
+                )
+        for i in range(2):
+            own_w1.append(
+                pltpu.make_async_copy(
+                    head_cols(2 * g + i, head_a if g == 0 else 3 - head_a),
+                    w1.at[g, 0, :, pl.ds(i * L, L)],
+                    lsem.at[6 + 2 * g + i],
+                )
+            )
+    for c in own_w1:
+        c.start()
+
+    got(gpos.at[pl.ds(1, 7)], 1)
+    got(etile.at[pl.ds(1, 3)], 2)
     x_part = jnp.zeros((16, B), F32)
     squares = jnp.zeros((1, B), F32)
-    for j in range(Y):
-        block = sgath[j * T : (j + 1) * T].astype(F32).reshape(L, B)
-        squares = squares + jnp.sum(block * block, axis=0, keepdims=True)
-        part = (transposed(block) * gains[j, 0:1, :]).astype(BF16)
+    scaled = []
+    for k in range(7):
+        if k == 0:
+            got(sgath.at[0, pl.ds(0, T - 1)], 16)
+        else:
+            got(sgath.at[k], 16 + k)
+        block = sgath[k].astype(F32).reshape(L, B)
+        part = (transposed(block) * gpos[k, 0:1, :]).astype(BF16)
         scaled.append(part)
-        x_part = x_part + lax.dot_general(
-            etile[j], part, (((1,), (1,)), ((), ())), preferred_element_type=F32
-        )
-    row16 = lax.broadcasted_iota(jnp.int32, (16, B), 0)
-    xz[z] = jnp.where(row16 == 8, squares, x_part)
-    for off in (4, 3, 5, 2, 6, 1, 7):
-        if off < Z:
-            zz = lax.rem(z + off, Z)
-            put(xz.at[z], xz.at[z], 4, (zz * Y + y, tp))
+        if k < 4:
+            squares = squares + jnp.sum(block * block, axis=0, keepdims=True)
+            x_part = x_part + lax.dot_general(
+                etile[k], part, (((1,), (1,)), ((), ())), preferred_element_type=F32
+            )
+        if k == 3:
+            row16 = lax.broadcasted_iota(jnp.int32, (16, B), 0)
+            xslot = lax.div(z, 2) * (Y // 2) + lax.div(y, 2)
+            xz[xslot] = jnp.where(row16 == 8, squares, x_part)
+            for i in (2, 1, 3, 0):
+                for j in (1, 0):
+                    if i or j:
+                        zz, yy = lax.rem(z + 2 * i, Z), lax.rem(y + 2 * j, Y)
+                        put(xz.at[xslot], xz.at[xslot], 4, (zz * Y + yy, tp))
 
     for c in own_w1:
         c.wait()
-    got(w1.at[pl.ds(0, Y - 1)], 3)
-    proj = jnp.zeros((B, 4 * L), F32)
-    for j in range(Y):
-        proj = proj + jnp.dot(scaled[j], w1[j], preferred_element_type=F32)
+    got(w1.at[:, pl.ds(1, 3)], 3)
+    proj = []
+    for g, members in groups:
+        total = jnp.zeros((B, 2 * L), F32)
+        for slot, k in enumerate(members):
+            total = total + jnp.dot(scaled[k], w1[g, slot], preferred_element_type=F32)
+        proj += [total[:, 0:L], total[:, L : 2 * L]]
     low = lax.broadcasted_iota(jnp.int32, (B // 8, 8, L), 1) < 4
 
     def pair_tiles(a, b):
@@ -244,7 +291,7 @@
             jnp.where(low, pltpu.roll(a, 4, 1), b),
         )
 
-    pq, pk, pv, pg = [proj[:, m * L : (m + 1) * L].reshape(B // 8, 8, L) for m in range(4)]
+    pq, pk, pv, pg = [p.reshape(B // 8, 8, L) for p in proj]
     even_a, odd_a = pair_tiles(pq, pk)
     even_b, odd_b = pair_tiles(pv, pg)
     s2[:, 0] = jnp.concatenate([even_a, even_b], axis=1).astype(BF16)
@@ -293,9 +340,12 @@
     row_id = lax.broadcasted_iota(jnp.int32, (16, 1), 0)
     acts = []
     for h in range(HEADS_DEV):
-        total = r2[h].astype(F32)
-        for j in range(1, Z):
-            total = total + r2[j * Y + h].astype(F32)
+        here = [
+            [n for n in range(N) if (n // Y % 2) * 2 + n % 2 == want] for want in (h, 3 - h)
+        ]
+        qk = [r2[n, 0:8, :].astype(F32) for n in here[0]]
+        vg = [r2[n, 8:16, :].astype(F32) for n in here[1]]
+        total = jnp.concatenate([added(qk), added(vg)], axis=0)
         a = silu(total * cols[:, 8:9])
         inv = lax.rsqrt(jnp.sum(a * a, axis=1, keepdims=True) + EPS)
         norm = jnp.where(row_id < 4, inv * L ** (-0.5), jnp.where(row_id < 8, inv, 1.0))
@@ -337,7 +387,8 @@
             wut[i * L : (i + 1) * L, j * L : (j + 1) * L] = transposed(
                 wu[j, :, i * L : (i + 1) * L].astype(F32)
             ).astype(BF16)
-        gcol[j] = transposed(jnp.broadcast_to(gains[j, 1:2, :], (B, L)))
+    for slot, yy in ((0, y), (2, ya), (5, yb), (7, lax.rem(y + 2, Y))):
+        gcol[yy] = transposed(jnp.broadcast_to(gpos[slot, 1:2, :], (B, L)))
     got(hall.at[pl.ds(0, N - 1)], 7)
     heads = hall[...].astype(F32).reshape(N // 2, 2, 2, 8, L)
     attn = jnp.zeros((L, B), F32)
@@ -413,10 +464,12 @@
     final = middle.astype(F32) + mixed * (factor2 * factor2)
     out_ref[...] = final.astype(BF16)
 
-    sent(sgath.at[pl.ds(0, PL - 1)], 0)
-    sent(gains.at[pl.ds(0, Y - 1)], 1)
-    sent(etile.at[pl.ds(0, Y - 1)], 2)
-    sent(w1.at[pl.ds(0, Y - 1)], 3)
+    sent(sgath.at[0, pl.ds(0, T - 1)], 16)
+    for k in range(1, 7):
+        sent(sgath.at[k], 16 + k)
+    sent(gpos.at[pl.ds(1, 7)], 1)
+    sent(etile.at[pl.ds(1, 3)], 2)
+    sent(w1.at[:, pl.ds(1, 3)], 3)
     sent(xz.at[pl.ds(0, Z - 1)], 4)
     sent(r2.at[pl.ds(0, N - 1)], 5)
     sent(wu.at[pl.ds(0, Y - 1)], 6)
@@ -484,10 +537,10 @@
             pltpu.VMEM((ROWS, HEADS_DEV, L, L), F32),
             pltpu.VMEM((4, L, 4 * L), BF16),
             pltpu.VMEM((4 * L, L), BF16),
-            pltpu.VMEM((Y, 8, L), F32),
-            pltpu.VMEM((Y, 16, L), BF16),
-            pltpu.VMEM((PL, DT, B), BF16),
-            pltpu.VMEM((Y, L, 4 * L), BF16),
+            pltpu.VMEM((8, 8, L), F32),
+            pltpu.VMEM((4, 16, L), BF16),
+            pltpu.VMEM((7, T, DT, B), BF16),
+            pltpu.VMEM((2, 4, L, 2 * L), BF16),
             pltpu.VMEM((Z, 16, B), F32),
             pltpu.VMEM((N // 2, 2, 16, L), BF16),
             pltpu.VMEM((N, 16, L), BF16),
@@ -509,8 +562,8 @@
             pltpu.VMEM((4 * L, 4 * L), BF16),
             pltpu.VMEM((Y, L, B), F32),
             pltpu.SemaphoreType.DMA((24,)),
-            pltpu.SemaphoreType.DMA((16,)),
-            pltpu.SemaphoreType.DMA((16,)),
+            pltpu.SemaphoreType.DMA((24,)),
+            pltpu.SemaphoreType.DMA((24,)),
         ],
         compiler_params=pltpu.CompilerParams(
             collective_id=0,

time: 65 us -> 62.3 us (0.958)
  Pallas kernels: 64.2 us -> 61.6 us
    pallas_call x1, Pallas kernels: 63.2 us -> 60.6 us  [shards(): pl.pallas_call(functools.partial(layer_kernel, Z, T), out_shape=(pltpu.VM...]
where the time goes in v4:
time: 62.3 us; the launch traced here: 62.2 us
  Pallas kernels  61.6 us (99%)
  between operations  0.64 us (1%)
    pallas_call x1, Pallas kernels, shards(): pl.pallas_call(functools.partial(layer_kernel, Z, T), out_shape=(pltpu.VM...  60.6 us

profile of v4, /device:TPU:1, one launch (start us, length us, event | category | flops | bytes accessed | tf_op | source)
XLA Modules:
  0.0 62.2 jit_solution(8460327806697946985)
XLA Ops:
  0.6 60.6 %shard_map.167 = (bf16[16,128]{1,0:T(8,128)(2,1)S(1)}, f32[4,4,128,128]{3,2,1,0:T(8,128)S(1)}) custom-call(bf16[16,128]{1,0:T(8,128)(2,1)} %bitcast.7, f32[1,128]{1,0:T(1,128)} %bitcast.10, f32[1,128]{1,0:T(1,128)} %bitcast.11, f32[1,128]{1,0:T(1,128)} %bitcast.12, bf16[4,128]{1,0:T(4,128)(2,1)} %bitcast.8, bf16[4,128]{1,0:T(4,128)(2,1)} %bitcast.9, ...), custom_call_target="tpu_custom_call" | custom-call | tf_op jit(solution)/shard_map/pallas_call | solution.py:520
  61.2 1.0 %shard_map.168 = (bf16[16,128]{1,0:T(8,128)(2,1)}, f32[4,4,128,128]{3,2,1,0:T(8,128)}) custom-call(bf16[16,128]{1,0:T(8,128)(2,1)S(1)} %get-tuple-element.6.layer_in, f32[4,4,128,128]{3,2,1,0:T(8,128)S(1)} %get-tuple-element.7.state_in), custom_call_target="tpu_custom_call" | custom-call | tf_op jit(solution)/shard_map/pallas_call | solution.py:591

commit v5 on v4

--- a/solution.py
+++ b/solution.py
@@ -66,7 +66,7 @@
     decay_shift_ref,
     state,
     w_in,
-    wo,
+    wof,
     gpos,
     etile,
     sgath,
@@ -87,10 +87,10 @@
     hall7,
     d8,
     r8,
-    wot,
     wut,
     wdt,
-    gcol,
+    gmix,
+    mids,
     lsem,
     ssem,
     rsem,
@@ -170,7 +170,8 @@
     ]
     for c in small:
         c.start()
-    load_out = pltpu.make_async_copy(wo_ref, wo, lsem.at[4])
+    own_out = wof.at[:, pl.ds(pl.multiple_of(y * L, L), L)]
+    load_out = pltpu.make_async_copy(wo_ref, own_out, lsem.at[4])
     load_state = pltpu.make_async_copy(state_ref, state, lsem.at[5])
     for c in loads:
         c.start()
@@ -201,22 +202,21 @@
     etile[0] = jnp.concatenate(
         [beta_ref[...].astype(F32), decay_ref[...].astype(F32), jnp.zeros((8, L), F32)], axis=0
     ).astype(BF16)
-    own_stream = stream_ref[...].astype(F32)
     sgath[0, tp] = stream_ref[...]
 
     with jax.named_scope("greeted"):
         pl.semaphore_wait(barrier, 7 * T - 1 + (Z - 3) + 1)
 
+    put(gpos.at[0], gpos.at[7], 1, (spot_far, tp))
     for k in (3, 6, 1, 2, 4, 5):
-        for t in tps:
-            put(sgath.at[0, tp], sgath.at[k, tp], 16 + k, (spots[k], t))
-    for t in tps[1:]:
-        put(sgath.at[0, tp], sgath.at[0, tp], 16, (kv, t))
-    for k in range(1, 7):
         put(gpos.at[0], gpos.at[k], 1, (spots[k], tp))
         if k < 4:
             put(etile.at[0], etile.at[k], 2, (spots[k], tp))
-    put(gpos.at[0], gpos.at[7], 1, (spot_far, tp))
+    for k in (3, 6, 1, 2, 4, 5):
+        for i in (4, 3, 5, 2, 6, 1, 7, 0):
+            put(sgath.at[0, tp], sgath.at[k, tp], 16 + k, (spots[k], tps[i]))
+    for i in (4, 3, 5, 2, 6, 1, 7):
+        put(sgath.at[0, tp], sgath.at[0, tp], 16, (kv, tps[i]))
     for c in loads:
         c.wait()
 
@@ -250,15 +250,15 @@
     got(etile.at[pl.ds(1, 3)], 2)
     x_part = jnp.zeros((16, B), F32)
     squares = jnp.zeros((1, B), F32)
-    scaled = []
-    for k in range(7):
+    scaled = {}
+    for k in (0, 1, 2, 3, 4, 5, 6):
         if k == 0:
             got(sgath.at[0, pl.ds(0, T - 1)], 16)
         else:
             got(sgath.at[k], 16 + k)
         block = sgath[k].astype(F32).reshape(L, B)
         part = (transposed(block) * gpos[k, 0:1, :]).astype(BF16)
-        scaled.append(part)
+        scaled[k] = part
         if k < 4:
             squares = squares + jnp.sum(block * block, axis=0, keepdims=True)
             x_part = x_part + lax.dot_general(
@@ -283,9 +283,8 @@
         for slot, k in enumerate(members):
             total = total + jnp.dot(scaled[k], w1[g, slot], preferred_element_type=F32)
         proj += [total[:, 0:L], total[:, L : 2 * L]]
-    low = lax.broadcasted_iota(jnp.int32, (B // 8, 8, L), 1) < 4
-
     def pair_tiles(a, b):
+        low = lax.broadcasted_iota(jnp.int32, a.shape, 1) < 4
         return (
             jnp.where(low, a, pltpu.roll(b, 4, 1)),
             jnp.where(low, pltpu.roll(a, 4, 1), b),
@@ -301,14 +300,10 @@
     )
     r2[kv] = s2[lax.div(kv, 2), lax.rem(kv, 2)]
 
-    def up_cols(yy):
-        return wu_ref.at[:, pl.ds(pl.multiple_of(yy * 4 * L, L), 4 * L)]
-
-    own_up = pltpu.make_async_copy(up_cols(y), wu.at[y], lsem.at[10])
-    own_up.start()
+    for t in tps:
+        put(sgath.at[0, tp], sgath.at[7, tp], 23, (spot_far, t))
     for off in (2, 1, 3):
-        yy = lax.rem(y + off, Y)
-        put(up_cols(yy), wu.at[y], 6, (z * Y + yy, tp))
+        put(wo_ref, own_out, 0, (z * Y + lax.rem(y + off, Y), tp))
 
     for c in late:
         c.wait()
@@ -364,22 +359,65 @@
             rows_f[0, 4 * h + r : 4 * h + r + 1, :] = jnp.sum(new * q_col, axis=0, keepdims=True)
     readout = rows_f[0]
     readout = readout * lax.rsqrt(jnp.mean(readout * readout, axis=1, keepdims=True) + EPS)
-    hall[kv] = (readout * head_gain_ref[...] * rows_f[1]).astype(BF16)
-
-    each_peer(N, kv, lambda p: put(hall.at[kv], hall.at[kv], 7, kv_dev(p)))
-
-    def down_rows(yy):
-        return wd_ref.at[pl.ds(pl.multiple_of(yy * 4 * L, L), 4 * L), :]
-
-    own_down = pltpu.make_async_copy(down_rows(y), wd.at[y], lsem.at[12])
-    own_down.start()
+    hall[z] = (readout * head_gain_ref[...] * rows_f[1]).astype(BF16)
+
+    offs = (4, 3, 5, 2, 6, 1, 7)
+    for off in offs:
+        put(hall.at[z], hall.at[z], 7, (lax.rem(z + off, Z) * Y + y, tp))
+
+    def up_cols(yy):
+        return wu_ref.at[:, pl.ds(pl.multiple_of(yy * 4 * L, L), 4 * L)]
+
+    own_up = pltpu.make_async_copy(up_cols(y), wu.at[y], lsem.at[10])
+    own_up.start()
     for off in (2, 1, 3):
         yy = lax.rem(y + off, Y)
-        put(down_rows(yy), wd.at[y], 8, (z * Y + yy, tp))
-
+        put(up_cols(yy), wu.at[y], 6, (z * Y + yy, tp))
+
+    got(sgath.at[7], 23)
+    row_mid = (tp * Y + y) * ROWS
+    sel_row = lax.broadcasted_iota(jnp.int32, (16, B), 0)
+    sel_lane = lax.broadcasted_iota(jnp.int32, (16, B), 1)
+    mid = jnp.zeros((16, L), F32)
+    for slot, yy in ((0, y), (2, ya), (5, yb), (7, lax.rem(y + 2, Y))):
+        gmix[yy] = gpos[slot]
+        pick = (lax.div(sel_row, 4) == yy) & (sel_lane == row_mid + lax.rem(sel_row, 4))
+        mid = mid + lax.dot_general(
+            jnp.where(pick, 1.0, 0.0).astype(BF16),
+            sgath[slot].reshape(L, B),
+            (((1,), (1,)), ((), ())),
+            preferred_element_type=F32,
+        )
     load_out.wait()
-    for i in range(HEADS_DEV):
-        wot[:, i * L : (i + 1) * L] = transposed(wo[i * L : (i + 1) * L, :].astype(F32)).astype(BF16)
+    got(wof.at[:, pl.ds(0, 3 * L)], 0)
+
+    got(hall.at[pl.ds(0, Z - 1)], 7)
+    heads = hall[...].astype(F32).reshape(Z // 2, 2, 2, 8, L)
+    attn = jnp.zeros((Z * ROWS, 4 * L), F32)
+    for c in range(2):
+        h_even, h_odd = pair_tiles(heads[:, 0, c], heads[:, 1, c])
+        for i, hh in ((2 * c, h_even), (2 * c + 1, h_odd)):
+            attn = attn + jnp.dot(
+                hh.reshape(Z * ROWS, L).astype(BF16),
+                wof[i * L : (i + 1) * L, :],
+                preferred_element_type=F32,
+            )
+    a_d = [attn[:, d * L : (d + 1) * L].reshape(Z // 2, 8, L) for d in range(4)]
+    even_a, odd_a = pair_tiles(a_d[0], a_d[1])
+    even_b, odd_b = pair_tiles(a_d[2], a_d[3])
+    a4[:, 0] = jnp.concatenate([even_a, even_b], axis=1).astype(BF16)
+    a4[:, 1] = jnp.concatenate([odd_a, odd_b], axis=1).astype(BF16)
+    for i in offs:
+        put(a4.at[lax.div(tps[i], 2), lax.rem(tps[i], 2)], r4.at[tp], 9, (kv, tps[i]))
+    r4[tp] = a4[lax.div(tp, 2), lax.rem(tp, 2)]
+    got(r4.at[pl.ds(0, T - 1)], 9)
+    mid = mid + added([r4[j].astype(F32) for j in range(T)])
+
+    slot_mid = tp * Y + y
+    mgath[slot_mid] = mid.astype(BF16)
+    each_peer(
+        PL, me_p, lambda p: put(mgath.at[slot_mid], mgath.at[slot_mid], 10, plane_dev(p))
+    )
     own_up.wait()
     got(wu.at[pl.ds(0, Y - 1)], 6)
     for j in range(Y):
@@ -387,53 +425,53 @@
             wut[i * L : (i + 1) * L, j * L : (j + 1) * L] = transposed(
                 wu[j, :, i * L : (i + 1) * L].astype(F32)
             ).astype(BF16)
-    for slot, yy in ((0, y), (2, ya), (5, yb), (7, lax.rem(y + 2, Y))):
-        gcol[yy] = transposed(jnp.broadcast_to(gpos[slot, 1:2, :], (B, L)))
-    got(hall.at[pl.ds(0, N - 1)], 7)
-    heads = hall[...].astype(F32).reshape(N // 2, 2, 2, 8, L)
-    attn = jnp.zeros((L, B), F32)
+    got(mgath.at[pl.ds(0, PL - 1)], 10)
+    pairs = mgath[...].astype(F32).reshape(N // 2, 2, 2, 8, L)
+    up = jnp.zeros((4 * L, B), F32)
+    middles = []
     for c in range(2):
-        h_even, h_odd = pair_tiles(heads[:, 0, c], heads[:, 1, c])
-        for i, hh in ((2 * c, h_even), (2 * c + 1, h_odd)):
-            attn = attn + lax.dot_general(
-                wot[:, i * L : (i + 1) * L],
-                hh.reshape(B, L).astype(BF16),
-                (((1,), (1,)), ((), ())),
-                preferred_element_type=F32,
-            )
-    a4[...] = attn.reshape(T, DT, B).astype(BF16)
-    each_peer(T, tp, lambda p: put(a4.at[p], r4.at[tp], 9, (kv, p)))
-    r4[tp] = a4[tp]
-    got(r4.at[pl.ds(0, T - 1)], 9)
-    attn_mine = r4[0].astype(F32)
-    for j in range(1, T):
-        attn_mine = attn_mine + r4[j].astype(F32)
-    middle = (own_stream + attn_mine).astype(BF16)
-
-    mgath[me_p] = middle
-    each_peer(PL, me_p, lambda p: put(mgath.at[me_p], mgath.at[me_p], 10, plane_dev(p)))
-    got(mgath.at[pl.ds(0, PL - 1)], 10)
-    up = jnp.zeros((4 * L, B), F32)
-    squares2 = jnp.zeros((1, B), F32)
-    for j in range(Y):
-        block = mgath[j * T : (j + 1) * T].astype(F32).reshape(L, B)
-        squares2 = squares2 + jnp.sum(block * block, axis=0, keepdims=True)
-        part = (block * gcol[j]).astype(BF16)
-        up = up + jnp.dot(wut[:, j * L : (j + 1) * L], part, preferred_element_type=F32)
+        middles += pair_tiles(pairs[:, 0, c], pairs[:, 1, c])
+    middles = [m.reshape(B, L) for m in middles]
+    for d in range(Y):
+        up = up + lax.dot_general(
+            wut[:, d * L : (d + 1) * L],
+            (middles[d] * gmix[d, 1:2, :]).astype(BF16),
+            (((1,), (1,)), ((), ())),
+            preferred_element_type=F32,
+        )
     u6[...] = up.astype(BF16).reshape(Z, 4 * L // Z, B)
-    sq[z] = jnp.broadcast_to(squares2, (8, B))
-    offs = [o for o in (4, 3, 5, 2, 6, 1, 7) if o < Z]
     for off in offs:
         zz = lax.rem(z + off, Z)
         put(u6.at[zz], r6.at[z], 11, (zz * Y + y, tp))
     r6[z] = u6[z]
-    own_down.wait()
-    got(wd.at[pl.ds(0, Y - 1)], 8)
-    for j in range(Y):
-        for i in range(4):
-            wdt[j * L : (j + 1) * L, i * L : (i + 1) * L] = transposed(
-                wd[j, i * L : (i + 1) * L, :].astype(F32)
-            ).astype(BF16)
+    def down_rows(yy):
+        return wd_ref.at[pl.ds(pl.multiple_of(yy * 4 * L, L), 4 * L), :]
+
+    own_down = pltpu.make_async_copy(down_rows(y), wd.at[y], lsem.at[12])
+    own_down.start()
+    for off in (2, 1, 3):
+        yy = lax.rem(y + off, Y)
+        put(down_rows(yy), wd.at[y], 8, (z * Y + yy, tp))
+
+    squares2 = jnp.zeros((8, B), F32)
+    for d in range(Y):
+        mids[d] = middles[d].astype(BF16)
+        squares2 = squares2 + lax.dot_general(
+            jnp.ones((8, L), F32),
+            middles[d] * middles[d],
+            (((1,), (1,)), ((), ())),
+            preferred_element_type=F32,
+            precision=lax.Precision.HIGHEST,
+        )
+    sq[z] = squares2
+    own_row = lax.broadcasted_iota(jnp.int32, (DT, L), 0) + tp * DT
+    own_lane = lax.broadcasted_iota(jnp.int32, (DT, L), 1)
+    middle = lax.dot_general(
+        jnp.where(own_row == own_lane, 1.0, 0.0).astype(BF16),
+        mids[y],
+        (((1,), (1,)), ((), ())),
+        preferred_element_type=F32,
+    )
     got(r6.at[pl.ds(0, Z - 1)], 11)
     up_mine = r6[0].astype(F32)
     for j in range(1, Z):
@@ -446,24 +484,32 @@
     for off in offs:
         zz = lax.rem(z + off, Z)
         put(sq.at[z], sq.at[z], 12, (zz * Y + y, tp))
+    own_down.wait()
+    got(wd.at[pl.ds(0, Y - 1)], 8)
+    for j in range(Y):
+        for i in range(4):
+            wdt[j * L : (j + 1) * L, i * L : (i + 1) * L] = transposed(
+                wd[j, i * L : (i + 1) * L, :].astype(F32)
+            ).astype(BF16)
     got(hall7.at[pl.ds(0, Z - 1)], 13)
-    down = jnp.dot(wdt[...], hall7[...].reshape(4 * L, B), preferred_element_type=F32)
-    d8[...] = down.reshape(PL, DT, B).astype(BF16)
-    each_peer(PL, me_p, lambda p: put(d8.at[p], r8.at[me_p], 14, plane_dev(p)))
+    hid = hall7[...].reshape(4 * L, B)
+    for off in (2, 1, 3, 0):
+        yy = lax.rem(y + off, Y)
+        first = yy * T
+        down = jnp.dot(
+            wdt[pl.ds(pl.multiple_of(yy * L, L), L), :], hid, preferred_element_type=F32
+        )
+        d8[pl.ds(first, T)] = down.reshape(T, DT, B).astype(BF16)
+        for i in (4, 3, 5, 2, 6, 1, 7, 0):
+            if off or i:
+                t = tps[i]
+                put(d8.at[first + t], r8.at[me_p], 14, (z * Y + yy, t))
     r8[me_p] = d8[me_p]
     got(sq.at[pl.ds(0, Z - 1)], 12)
     total2 = sq[0, 0:1, :]
     for j in range(1, Z):
         total2 = total2 + sq[j, 0:1, :]
     factor2 = lax.rsqrt(total2 / D + EPS)
-    got(r8.at[pl.ds(0, PL - 1)], 14)
-    parts = [r8[j].astype(F32) for j in range(4)]
-    for j in range(4, PL):
-        parts[j % 4] = parts[j % 4] + r8[j].astype(F32)
-    mixed = (parts[0] + parts[1]) + (parts[2] + parts[3])
-    final = middle.astype(F32) + mixed * (factor2 * factor2)
-    out_ref[...] = final.astype(BF16)
-
     sent(sgath.at[0, pl.ds(0, T - 1)], 16)
     for k in range(1, 7):
         sent(sgath.at[k], 16 + k)
@@ -473,13 +519,22 @@
     sent(xz.at[pl.ds(0, Z - 1)], 4)
     sent(r2.at[pl.ds(0, N - 1)], 5)
     sent(wu.at[pl.ds(0, Y - 1)], 6)
-    sent(hall.at[pl.ds(0, N - 1)], 7)
+    sent(hall.at[pl.ds(0, Z - 1)], 7)
+    sent(wof.at[:, pl.ds(0, 3 * L)], 0)
+    sent(sgath.at[7], 23)
     sent(wd.at[pl.ds(0, Y - 1)], 8)
     sent(r4.at[pl.ds(0, T - 1)], 9)
     sent(mgath.at[pl.ds(0, PL - 1)], 10)
     sent(r6.at[pl.ds(0, Z - 1)], 11)
     sent(sq.at[pl.ds(0, Z - 1)], 12)
     sent(hall7.at[pl.ds(0, Z - 1)], 13)
+    got(r8.at[pl.ds(0, PL - 1)], 14)
+    parts = [r8[j].astype(F32) for j in range(4)]
+    for j in range(4, PL):
+        parts[j % 4] = parts[j % 4] + r8[j].astype(F32)
+    mixed = (parts[0] + parts[1]) + (parts[2] + parts[3])
+    final = middle + mixed * (factor2 * factor2)
+    out_ref[...] = final.astype(BF16)
     sent(r8.at[pl.ds(0, PL - 1)], 14)
 
 
@@ -536,19 +591,19 @@
             pltpu.SMEM((HEADS_DEV,), F32),
             pltpu.VMEM((ROWS, HEADS_DEV, L, L), F32),
             pltpu.VMEM((4, L, 4 * L), BF16),
-            pltpu.VMEM((4 * L, L), BF16),
+            pltpu.VMEM((4 * L, 4 * L), BF16),
             pltpu.VMEM((8, 8, L), F32),
             pltpu.VMEM((4, 16, L), BF16),
-            pltpu.VMEM((7, T, DT, B), BF16),
+            pltpu.VMEM((8, T, DT, B), BF16),
             pltpu.VMEM((2, 4, L, 2 * L), BF16),
             pltpu.VMEM((Z, 16, B), F32),
             pltpu.VMEM((N // 2, 2, 16, L), BF16),
             pltpu.VMEM((N, 16, L), BF16),
             pltpu.VMEM((2, 16, L), F32),
+            pltpu.VMEM((Z, 16, L), BF16),
+            pltpu.VMEM((Z // 2, 2, 16, L), BF16),
+            pltpu.VMEM((T, 16, L), BF16),
             pltpu.VMEM((N, 16, L), BF16),
-            pltpu.VMEM((T, DT, B), BF16),
-            pltpu.VMEM((T, DT, B), BF16),
-            pltpu.VMEM((PL, DT, B), BF16),
             pltpu.VMEM((Y, L, 4 * L), BF16),
             pltpu.VMEM((Y, 4 * L, L), BF16),
             pltpu.VMEM((Z, 8, B), F32),
@@ -557,10 +612,10 @@
             pltpu.VMEM((Z, 4 * L // Z, B), BF16),
             pltpu.VMEM((PL, DT, B), BF16),
             pltpu.VMEM((PL, DT, B), BF16),
-            pltpu.VMEM((L, 4 * L), BF16),
             pltpu.VMEM((4 * L, 4 * L), BF16),
             pltpu.VMEM((4 * L, 4 * L), BF16),
-            pltpu.VMEM((Y, L, B), F32),
+            pltpu.VMEM((Y, 8, L), F32),
+            pltpu.VMEM((Y, B, L), BF16),
             pltpu.SemaphoreType.DMA((24,)),
             pltpu.SemaphoreType.DMA((24,)),
             pltpu.SemaphoreType.DMA((24,)),

time: 62.3 us -> 59.8 us (0.960)
  Pallas kernels: 61.6 us -> 59 us
    pallas_call x1, Pallas kernels: 60.6 us -> 58 us  [shards(): pl.pallas_call(functools.partial(layer_kernel, Z, T), out_shape=(pltpu.VM...]
where the time goes in v5:
time: 59.8 us; the launch traced here: 59.7 us
  Pallas kernels  59 us (99%)
  between operations  0.64 us (1%)
    pallas_call x1, Pallas kernels, shards(): pl.pallas_call(functools.partial(layer_kernel, Z, T), out_shape=(pltpu.VM...  58 us

profile of v5, /device:TPU:1, one launch (start us, length us, event | category | flops | bytes accessed | tf_op | source)
XLA Modules:
  0.0 59.7 jit_solution(606663820123309382)
XLA Ops:
  0.6 58.0 %shard_map.167 = (bf16[16,128]{1,0:T(8,128)(2,1)S(1)}, f32[4,4,128,128]{3,2,1,0:T(8,128)S(1)}) custom-call(bf16[16,128]{1,0:T(8,128)(2,1)} %bitcast.7, f32[1,128]{1,0:T(1,128)} %bitcast.10, f32[1,128]{1,0:T(1,128)} %bitcast.11, f32[1,128]{1,0:T(1,128)} %bitcast.12, bf16[4,128]{1,0:T(4,128)(2,1)} %bitcast.8, bf16[4,128]{1,0:T(4,128)(2,1)} %bitcast.9, ...), custom_call_target="tpu_custom_call" | custom-call | tf_op jit(solution)/shard_map/pallas_call | solution.py:575
  58.7 1.0 %shard_map.168 = (bf16[16,128]{1,0:T(8,128)(2,1)}, f32[4,4,128,128]{3,2,1,0:T(8,128)}) custom-call(bf16[16,128]{1,0:T(8,128)(2,1)S(1)} %get-tuple-element.6.layer_in, f32[4,4,128,128]{3,2,1,0:T(8,128)S(1)} %get-tuple-element.7.state_in), custom_call_target="tpu_custom_call" | custom-call | tf_op jit(solution)/shard_map/pallas_call | solution.py:646

commit v6 on v5

--- a/solution.py
+++ b/solution.py
@@ -91,6 +91,7 @@
     wdt,
     gmix,
     mids,
+    all_sent,
     lsem,
     ssem,
     rsem,
@@ -133,7 +134,7 @@
         pltpu.make_async_remote_copy(
             src_ref=src,
             dst_ref=dst,
-            send_sem=ssem.at[k],
+            send_sem=ssem,
             recv_sem=rsem.at[k],
             device_id=dev,
             device_id_type=MESH,
@@ -143,15 +144,13 @@
         with jax.named_scope(f"got{k}"):
             pltpu.make_async_copy(ref, ref, rsem.at[k]).wait()
 
-    def sent(ref, k):
-        pltpu.make_async_copy(ref, ref, ssem.at[k]).wait()
 
     loads = [
-        pltpu.make_async_copy(w, w_in.at[m], lsem.at[m])
+        pltpu.make_async_copy(w, w_in.at[m], lsem.at[0])
         for m, w in enumerate((wq_ref, wk_ref, wv_ref, wg_ref))
     ]
     small = [
-        pltpu.make_async_copy(a, b, lsem.at[16 + i])
+        pltpu.make_async_copy(a, b, lsem.at[3 + i])
         for i, (a, b) in enumerate((
             (stream_hbm, stream_ref),
             (attn_gain_hbm, attn_gain_ref),
@@ -161,7 +160,7 @@
         ))
     ]
     late = [
-        pltpu.make_async_copy(a, b, lsem.at[21 + i])
+        pltpu.make_async_copy(a, b, lsem.at[3 + i])
         for i, (a, b) in enumerate((
             (head_gain_hbm, head_gain_ref),
             (decay_log_hbm, decay_log_ref),
@@ -171,14 +170,12 @@
     for c in small:
         c.start()
     own_out = wof.at[:, pl.ds(pl.multiple_of(y * L, L), L)]
-    load_out = pltpu.make_async_copy(wo_ref, own_out, lsem.at[4])
-    load_state = pltpu.make_async_copy(state_ref, state, lsem.at[5])
+    load_out = pltpu.make_async_copy(wo_ref, own_out, lsem.at[1])
+    load_state = pltpu.make_async_copy(state_ref, state, lsem.at[2])
     for c in loads:
         c.start()
     load_out.start()
     load_state.start()
-    for c in late:
-        c.start()
 
     barrier = pltpu.get_barrier_semaphore()
 
@@ -197,6 +194,8 @@
 
     for c in small:
         c.wait()
+    for c in late:
+        c.start()
     gpos[0] = jnp.broadcast_to(attn_gain_ref[...], (8, L))
     gpos[0, 1:2, :] = mixer_gain_ref[...]
     etile[0] = jnp.concatenate(
@@ -214,17 +213,16 @@
             put(etile.at[0], etile.at[k], 2, (spots[k], tp))
     for k in (3, 6, 1, 2, 4, 5):
         for i in (4, 3, 5, 2, 6, 1, 7, 0):
-            put(sgath.at[0, tp], sgath.at[k, tp], 16 + k, (spots[k], tps[i]))
+            put(sgath.at[0, tp], sgath.at[k, tp], (16 if k < 4 else 17), (spots[k], tps[i]))
     for i in (4, 3, 5, 2, 6, 1, 7):
-        put(sgath.at[0, tp], sgath.at[0, tp], 16, (kv, tps[i]))
-    for c in loads:
-        c.wait()
+        put(sgath.at[0, tp], sgath.at[0, tp], 15, (kv, tps[i]))
+    pltpu.make_async_copy(w_in, w_in, lsem.at[0]).wait()
 
     def head_cols(m, h):
         return w_in.at[m, :, pl.ds(pl.multiple_of(h * L, L), L)]
 
-    own_w1 = []
-    for g, members in groups:
+    def send_weights(g):
+        members = groups[g][1]
         for slot in (3, 1, 2):
             h = heads_a[slot]
             h = h if g == 0 else 3 - h
@@ -232,20 +230,19 @@
                 put(
                     head_cols(2 * g + i, h),
                     w1.at[g, slot, :, pl.ds(i * L, L)],
-                    3,
+                    3 if g == 0 else 19,
                     (spots[members[slot]], tp),
                 )
+
+    send_weights(0)
+    for g in range(2):
         for i in range(2):
-            own_w1.append(
-                pltpu.make_async_copy(
-                    head_cols(2 * g + i, head_a if g == 0 else 3 - head_a),
-                    w1.at[g, 0, :, pl.ds(i * L, L)],
-                    lsem.at[6 + 2 * g + i],
-                )
-            )
-    for c in own_w1:
-        c.start()
-
+            pltpu.make_async_copy(
+                head_cols(2 * g + i, head_a if g == 0 else 3 - head_a),
+                w1.at[g, 0, :, pl.ds(i * L, L)],
+                lsem.at[0],
+            ).start()
+    send_weights(1)
     got(gpos.at[pl.ds(1, 7)], 1)
     got(etile.at[pl.ds(1, 3)], 2)
     x_part = jnp.zeros((16, B), F32)
@@ -253,9 +250,11 @@
     scaled = {}
     for k in (0, 1, 2, 3, 4, 5, 6):
         if k == 0:
-            got(sgath.at[0, pl.ds(0, T - 1)], 16)
-        else:
-            got(sgath.at[k], 16 + k)
+            got(sgath.at[0, pl.ds(0, T - 1)], 15)
+        elif k == 1:
+            got(sgath.at[pl.ds(1, 3)], 16)
+        elif k == 4:
+            got(sgath.at[pl.ds(4, 3)], 17)
         block = sgath[k].astype(F32).reshape(L, B)
         part = (transposed(block) * gpos[k, 0:1, :]).astype(BF16)
         scaled[k] = part
@@ -267,18 +266,17 @@
         if k == 3:
             row16 = lax.broadcasted_iota(jnp.int32, (16, B), 0)
             xslot = lax.div(z, 2) * (Y // 2) + lax.div(y, 2)
-            xz[xslot] = jnp.where(row16 == 8, squares, x_part)
+            xz[xslot] = jnp.where(row16 == 8, squares, x_part).astype(BF16)
             for i in (2, 1, 3, 0):
                 for j in (1, 0):
                     if i or j:
                         zz, yy = lax.rem(z + 2 * i, Z), lax.rem(y + 2 * j, Y)
                         put(xz.at[xslot], xz.at[xslot], 4, (zz * Y + yy, tp))
 
-    for c in own_w1:
-        c.wait()
-    got(w1.at[:, pl.ds(1, 3)], 3)
+    pltpu.make_async_copy(w1.at[:, 0], w1.at[:, 0], lsem.at[0]).wait()
     proj = []
     for g, members in groups:
+        got(w1.at[g, pl.ds(1, 3)], 3 if g == 0 else 19)
         total = jnp.zeros((B, 2 * L), F32)
         for slot, k in enumerate(members):
             total = total + jnp.dot(scaled[k], w1[g, slot], preferred_element_type=F32)
@@ -301,16 +299,14 @@
     r2[kv] = s2[lax.div(kv, 2), lax.rem(kv, 2)]
 
     for t in tps:
-        put(sgath.at[0, tp], sgath.at[7, tp], 23, (spot_far, t))
+        put(sgath.at[0, tp], sgath.at[7, tp], 18, (spot_far, t))
     for off in (2, 1, 3):
         put(wo_ref, own_out, 0, (z * Y + lax.rem(y + off, Y), tp))
 
     for c in late:
         c.wait()
     got(xz.at[pl.ds(0, Z - 1)], 4)
-    x_all = xz[0]
-    for j in range(1, Z):
-        x_all = x_all + xz[j]
+    x_all = added([xz[j].astype(F32) for j in range(Z)])
     fac = lax.rsqrt(x_all[8:9] / D + EPS)
     xf = x_all * fac
     dlog = jnp.zeros((16, B), F32)
@@ -330,6 +326,11 @@
         mine = jnp.where(lane_group == m, rolled, mine)
     cols = transposed(jnp.concatenate([mine, jnp.zeros((L - 16, B), F32)], axis=0))[0:16]
 
+    head_of = lax.div(lax.broadcasted_iota(jnp.int32, (16, L), 0), 4)
+    lane16 = lax.broadcasted_iota(jnp.int32, (16, L), 1)
+    beta16 = jnp.sum(jnp.where(lane16 == head_of, cols, 0.0), axis=1, keepdims=True)
+    decay16 = jnp.sum(jnp.where(lane16 == 4 + head_of, cols, 0.0), axis=1, keepdims=True)
+
     got(r2.at[pl.ds(0, N - 1)], 5)
     load_state.wait()
     row_id = lax.broadcasted_iota(jnp.int32, (16, 1), 0)
@@ -345,21 +346,25 @@
         inv = lax.rsqrt(jnp.sum(a * a, axis=1, keepdims=True) + EPS)
         norm = jnp.where(row_id < 4, inv * L ** (-0.5), jnp.where(row_id < 8, inv, 1.0))
         acts.append(a * norm)
-        rows_f[1, 4 * h : 4 * h + 4, :] = a[12:16]
+        for n, lo in ((0, 0), (1, 4), (2, 8), (3, 12)):
+            rows_f[n, 4 * h : 4 * h + 4, :] = acts[h][lo : lo + 4]
     flipped = transposed(jnp.concatenate(acts + [jnp.zeros((L - 64, L), F32)], axis=0))
-    for h in range(HEADS_DEV):
-        for r in range(ROWS):
-            q_col = flipped[:, h * 16 + r : h * 16 + r + 1]
-            k_col = flipped[:, h * 16 + 4 + r : h * 16 + 5 + r]
-            kept = state[r, h] * cols[r : r + 1, 4 + h : 5 + h]
-            recalled = jnp.sum(kept * k_col, axis=0, keepdims=True)
-            corr = cols[r : r + 1, h : h + 1] * (acts[h][8 + r : 9 + r] - recalled)
-            new = kept + k_col * corr
-            next_ref[r, h] = new
-            rows_f[0, 4 * h + r : 4 * h + r + 1, :] = jnp.sum(new * q_col, axis=0, keepdims=True)
-    readout = rows_f[0]
+    pieces = [(h, r) for h in range(HEADS_DEV) for r in range(ROWS)]
+    for h, r in pieces:
+        at = h * 16 + r
+        own = state[r, h]
+        row = 4 * h + r
+        rows_f[4, row : row + 1, :] = jnp.sum(
+            own * flipped[:, at : at + 1], axis=0, keepdims=True
+        )
+        rows_f[5, row : row + 1, :] = jnp.sum(
+            own * flipped[:, at + 4 : at + 5], axis=0, keepdims=True
+        )
+    corr = beta16 * (rows_f[2] - decay16 * rows_f[5])
+    along = jnp.sum(rows_f[0] * rows_f[1], axis=1, keepdims=True)
+    readout = decay16 * rows_f[4] + along * corr
     readout = readout * lax.rsqrt(jnp.mean(readout * readout, axis=1, keepdims=True) + EPS)
-    hall[z] = (readout * head_gain_ref[...] * rows_f[1]).astype(BF16)
+    hall[z] = (readout * head_gain_ref[...] * rows_f[3]).astype(BF16)
 
     offs = (4, 3, 5, 2, 6, 1, 7)
     for off in offs:
@@ -368,13 +373,20 @@
     def up_cols(yy):
         return wu_ref.at[:, pl.ds(pl.multiple_of(yy * 4 * L, L), 4 * L)]
 
-    own_up = pltpu.make_async_copy(up_cols(y), wu.at[y], lsem.at[10])
+    own_up = pltpu.make_async_copy(up_cols(y), wu.at[y], lsem.at[0])
     own_up.start()
     for off in (2, 1, 3):
         yy = lax.rem(y + off, Y)
         put(up_cols(yy), wu.at[y], 6, (z * Y + yy, tp))
 
-    got(sgath.at[7], 23)
+    for h, r in pieces:
+        row = 4 * h + r
+        at = h * 16 + 4 + r
+        next_ref[r, h] = (
+            state[r, h] * decay16[row : row + 1] + flipped[:, at : at + 1] * corr[row : row + 1]
+        )
+
+    got(sgath.at[7], 18)
     row_mid = (tp * Y + y) * ROWS
     sel_row = lax.broadcasted_iota(jnp.int32, (16, B), 0)
     sel_lane = lax.broadcasted_iota(jnp.int32, (16, B), 1)
@@ -440,14 +452,16 @@
             preferred_element_type=F32,
         )
     u6[...] = up.astype(BF16).reshape(Z, 4 * L // Z, B)
-    for off in offs:
-        zz = lax.rem(z + off, Z)
-        put(u6.at[zz], r6.at[z], 11, (zz * Y + y, tp))
+    for zz in (4, 3, 5, 2, 6, 1, 7, 0):
+        @pl.when(z != zz)
+        def _(zz=zz):
+            put(u6.at[zz], r6.at[z], 11, (zz * Y + y, tp))
+
     r6[z] = u6[z]
     def down_rows(yy):
         return wd_ref.at[pl.ds(pl.multiple_of(yy * 4 * L, L), 4 * L), :]
 
-    own_down = pltpu.make_async_copy(down_rows(y), wd.at[y], lsem.at[12])
+    own_down = pltpu.make_async_copy(down_rows(y), wd.at[y], lsem.at[0])
     own_down.start()
     for off in (2, 1, 3):
         yy = lax.rem(y + off, Y)
@@ -478,12 +492,12 @@
         up_mine = up_mine + r6[j].astype(F32)
     hidden = jnp.square(jnp.maximum(up_mine, 0.0)).astype(BF16)
     hall7[z] = hidden
-    for off in offs:
-        zz = lax.rem(z + off, Z)
-        put(hall7.at[z], hall7.at[z], 13, (zz * Y + y, tp))
-    for off in offs:
-        zz = lax.rem(z + off, Z)
-        put(sq.at[z], sq.at[z], 12, (zz * Y + y, tp))
+    for ref, k in ((hall7, 13), (sq, 12)):
+        for zz in range(Z):
+            @pl.when(z != zz)
+            def _(ref=ref, k=k, zz=zz):
+                put(ref.at[z], ref.at[z], k, (zz * Y + y, tp))
+
     own_down.wait()
     got(wd.at[pl.ds(0, Y - 1)], 8)
     for j in range(Y):
@@ -493,41 +507,20 @@
             ).astype(BF16)
     got(hall7.at[pl.ds(0, Z - 1)], 13)
     hid = hall7[...].reshape(4 * L, B)
-    for off in (2, 1, 3, 0):
-        yy = lax.rem(y + off, Y)
-        first = yy * T
-        down = jnp.dot(
-            wdt[pl.ds(pl.multiple_of(yy * L, L), L), :], hid, preferred_element_type=F32
-        )
-        d8[pl.ds(first, T)] = down.reshape(T, DT, B).astype(BF16)
-        for i in (4, 3, 5, 2, 6, 1, 7, 0):
-            if off or i:
-                t = tps[i]
-                put(d8.at[first + t], r8.at[me_p], 14, (z * Y + yy, t))
+    for yy in (0, 1, 3, 2):
+        down = jnp.dot(wdt[yy * L : (yy + 1) * L, :], hid, preferred_element_type=F32)
+        d8[yy * T : (yy + 1) * T] = down.reshape(T, DT, B).astype(BF16)
+        for t in (1, 0, 3, 2, 7, 6, 5, 4):
+            @pl.when(me_p != yy * T + t)
+            def _(yy=yy, t=t):
+                put(d8.at[yy * T + t], r8.at[me_p], 14, (z * Y + yy, t))
+
     r8[me_p] = d8[me_p]
     got(sq.at[pl.ds(0, Z - 1)], 12)
     total2 = sq[0, 0:1, :]
     for j in range(1, Z):
         total2 = total2 + sq[j, 0:1, :]
     factor2 = lax.rsqrt(total2 / D + EPS)
-    sent(sgath.at[0, pl.ds(0, T - 1)], 16)
-    for k in range(1, 7):
-        sent(sgath.at[k], 16 + k)
-    sent(gpos.at[pl.ds(1, 7)], 1)
-    sent(etile.at[pl.ds(1, 3)], 2)
-    sent(w1.at[:, pl.ds(1, 3)], 3)
-    sent(xz.at[pl.ds(0, Z - 1)], 4)
-    sent(r2.at[pl.ds(0, N - 1)], 5)
-    sent(wu.at[pl.ds(0, Y - 1)], 6)
-    sent(hall.at[pl.ds(0, Z - 1)], 7)
-    sent(wof.at[:, pl.ds(0, 3 * L)], 0)
-    sent(sgath.at[7], 23)
-    sent(wd.at[pl.ds(0, Y - 1)], 8)
-    sent(r4.at[pl.ds(0, T - 1)], 9)
-    sent(mgath.at[pl.ds(0, PL - 1)], 10)
-    sent(r6.at[pl.ds(0, Z - 1)], 11)
-    sent(sq.at[pl.ds(0, Z - 1)], 12)
-    sent(hall7.at[pl.ds(0, Z - 1)], 13)
     got(r8.at[pl.ds(0, PL - 1)], 14)
     parts = [r8[j].astype(F32) for j in range(4)]
     for j in range(4, PL):
@@ -535,7 +528,7 @@
     mixed = (parts[0] + parts[1]) + (parts[2] + parts[3])
     final = middle + mixed * (factor2 * factor2)
     out_ref[...] = final.astype(BF16)
-    sent(r8.at[pl.ds(0, PL - 1)], 14)
+    pltpu.make_async_copy(all_sent, all_sent, ssem).wait()
 
 
 def hand_over(layer_in, state_in, layer_ref, state_ref, sems):
@@ -569,6 +562,16 @@
     down_weight,
 ):
     N, PL, B, DT = Z * Y, Y * T, Z * Y * ROWS, L // T
+    sent_tiles = (
+        3 * 3 * 32
+        + 12 * 8
+        + 7 + 3
+        + 7 * 8 - 1 + 8
+        + 7 + (N - 1)
+        + (Z - 1) + (T - 1) + (PL - 1)
+        + 2 * 4 * (Z - 1) + (Z - 1)
+        + (PL - 1)
+    )
     hbm = pl.BlockSpec(memory_space=pltpu.HBM)
     anywhere = pl.BlockSpec(memory_space=pl.ANY)
     vmem = pl.BlockSpec(memory_space=pltpu.VMEM)
@@ -596,10 +599,10 @@
             pltpu.VMEM((4, 16, L), BF16),
             pltpu.VMEM((8, T, DT, B), BF16),
             pltpu.VMEM((2, 4, L, 2 * L), BF16),
-            pltpu.VMEM((Z, 16, B), F32),
+            pltpu.VMEM((Z, 16, B), BF16),
             pltpu.VMEM((N // 2, 2, 16, L), BF16),
             pltpu.VMEM((N, 16, L), BF16),
-            pltpu.VMEM((2, 16, L), F32),
+            pltpu.VMEM((6, 16, L), F32),
             pltpu.VMEM((Z, 16, L), BF16),
             pltpu.VMEM((Z // 2, 2, 16, L), BF16),
             pltpu.VMEM((T, 16, L), BF16),
@@ -616,9 +619,10 @@
             pltpu.VMEM((4 * L, 4 * L), BF16),
             pltpu.VMEM((Y, 8, L), F32),
             pltpu.VMEM((Y, B, L), BF16),
-            pltpu.SemaphoreType.DMA((24,)),
-            pltpu.SemaphoreType.DMA((24,)),
-            pltpu.SemaphoreType.DMA((24,)),
+            pltpu.VMEM((sent_tiles, 16, L), BF16),
+            pltpu.SemaphoreType.DMA((8,)),
+            pltpu.SemaphoreType.DMA,
+            pltpu.SemaphoreType.DMA((20,)),
         ],
         compiler_params=pltpu.CompilerParams(
             collective_id=0,

time: 59.8 us -> 58.2 us (0.973)
  Pallas kernels: 59 us -> 57.5 us
    pallas_call x1, Pallas kernels: 58 us -> 56.5 us  [shards(): pl.pallas_call(functools.partial(layer_kernel, Z, T), out_shape=(pltpu.VM...]
where the time goes in v6:
time: 58.2 us; the launch traced here: 58.1 us
  Pallas kernels  57.5 us (99%)
  between operations  0.64 us (1%)
    pallas_call x1, Pallas kernels, shards(): pl.pallas_call(functools.partial(layer_kernel, Z, T), out_shape=(pltpu.VM...  56.5 us

profile of v6, /device:TPU:1, one launch (start us, length us, event | category | flops | bytes accessed | tf_op | source)
XLA Modules:
  0.0 58.1 jit_solution(13164395521531705372)
XLA Ops:
  0.6 56.5 %shard_map.167 = (bf16[16,128]{1,0:T(8,128)(2,1)S(1)}, f32[4,4,128,128]{3,2,1,0:T(8,128)S(1)}) custom-call(bf16[16,128]{1,0:T(8,128)(2,1)} %bitcast.7, f32[1,128]{1,0:T(1,128)} %bitcast.10, f32[1,128]{1,0:T(1,128)} %bitcast.11, f32[1,128]{1,0:T(1,128)} %bitcast.12, bf16[4,128]{1,0:T(4,128)(2,1)} %bitcast.8, bf16[4,128]{1,0:T(4,128)(2,1)} %bitcast.9, ...), custom_call_target="tpu_custom_call" | custom-call | tf_op jit(solution)/shard_map/pallas_call | solution.py:578
  57.1 1.0 %shard_map.168 = (bf16[16,128]{1,0:T(8,128)(2,1)}, f32[4,4,128,128]{3,2,1,0:T(8,128)}) custom-call(bf16[16,128]{1,0:T(8,128)(2,1)S(1)} %get-tuple-element.6.layer_in, f32[4,4,128,128]{3,2,1,0:T(8,128)S(1)} %get-tuple-element.7.state_in), custom_call_target="tpu_custom_call" | custom-call | tf_op jit(solution)/shard_map/pallas_call | solution.py:650

commit v7 on v6

--- a/solution.py
+++ b/solution.py
@@ -115,20 +115,9 @@
     heads_a = [head_a, (1 - pz) * 2 + py, pz * 2 + 1 - py, (1 - pz) * 2 + 1 - py]
     groups = ((0, (0, 1, 2, 3)), (1, (0, 4, 5, 6)))
     tps = [lax.rem(tp + i, T) for i in range(T)]
-
-    def plane_dev(p):
-        return (z * Y + lax.div(p, T), lax.rem(p, T))
-
-    def kv_dev(p):
-        return (p, tp)
-
-    def each_peer(n, me, act):
-        def step(i, c):
-            off = 1 + lax.rem(i + (n // 2 - 1), n - 1)
-            act(lax.rem(me + off, n))
-            return c
-
-        lax.fori_loop(0, n - 1, step, 0)
+    zs_ = [lax.rem(z + i, Z) for i in range(Z)]
+    ys_ = [lax.rem(y + i, Y) for i in range(Y)]
+    ys_half, ys_odd = [lax.div(v, 2) for v in ys_], [lax.rem(v, 2) for v in ys_]
 
     def put(src, dst, k, dev):
         pltpu.make_async_remote_copy(
@@ -293,9 +282,11 @@
     even_b, odd_b = pair_tiles(pv, pg)
     s2[:, 0] = jnp.concatenate([even_a, even_b], axis=1).astype(BF16)
     s2[:, 1] = jnp.concatenate([odd_a, odd_b], axis=1).astype(BF16)
-    each_peer(
-        N, kv, lambda p: put(s2.at[lax.div(p, 2), lax.rem(p, 2)], r2.at[kv], 5, kv_dev(p))
-    )
+    for dz in (4, 3, 5, 2, 6, 1, 7, 0):
+        for dy in (2, 1, 3, 0):
+            if dz or dy:
+                zz, yy = zs_[dz], ys_[dy]
+                put(s2.at[2 * zz + ys_half[dy], ys_odd[dy]], r2.at[kv], 5, (zz * Y + yy, tp))
     r2[kv] = s2[lax.div(kv, 2), lax.rem(kv, 2)]
 
     for t in tps:
@@ -367,8 +358,11 @@
     hall[z] = (readout * head_gain_ref[...] * rows_f[3]).astype(BF16)
 
     offs = (4, 3, 5, 2, 6, 1, 7)
-    for off in offs:
-        put(hall.at[z], hall.at[z], 7, (lax.rem(z + off, Z) * Y + y, tp))
+    for zz in (0, 1, 7, 2, 6, 3, 5, 4):
+        @pl.when(z != zz)
+        def _(zz=zz):
+            put(hall.at[z], hall.at[z], 7, (zz * Y + y, tp))
+
 
     def up_cols(yy):
         return wu_ref.at[:, pl.ds(pl.multiple_of(yy * 4 * L, L), 4 * L)]
@@ -379,14 +373,13 @@
         yy = lax.rem(y + off, Y)
         put(up_cols(yy), wu.at[y], 6, (z * Y + yy, tp))
 
+    got(sgath.at[7], 18)
     for h, r in pieces:
         row = 4 * h + r
         at = h * 16 + 4 + r
         next_ref[r, h] = (
             state[r, h] * decay16[row : row + 1] + flipped[:, at : at + 1] * corr[row : row + 1]
         )
-
-    got(sgath.at[7], 18)
     row_mid = (tp * Y + y) * ROWS
     sel_row = lax.broadcasted_iota(jnp.int32, (16, B), 0)
     sel_lane = lax.broadcasted_iota(jnp.int32, (16, B), 1)
@@ -427,9 +420,10 @@
 
     slot_mid = tp * Y + y
     mgath[slot_mid] = mid.astype(BF16)
-    each_peer(
-        PL, me_p, lambda p: put(mgath.at[slot_mid], mgath.at[slot_mid], 10, plane_dev(p))
-    )
+    for dy in (2, 1, 3, 0):
+        for i in (4, 3, 5, 2, 6, 1, 7, 0):
+            if dy or i:
+                put(mgath.at[slot_mid], mgath.at[slot_mid], 10, (z * Y + ys_[dy], tps[i]))
     own_up.wait()
     got(wu.at[pl.ds(0, Y - 1)], 6)
     for j in range(Y):
@@ -439,23 +433,25 @@
             ).astype(BF16)
     got(mgath.at[pl.ds(0, PL - 1)], 10)
     pairs = mgath[...].astype(F32).reshape(N // 2, 2, 2, 8, L)
-    up = jnp.zeros((4 * L, B), F32)
     middles = []
     for c in range(2):
         middles += pair_tiles(pairs[:, 0, c], pairs[:, 1, c])
     middles = [m.reshape(B, L) for m in middles]
-    for d in range(Y):
-        up = up + lax.dot_general(
-            wut[:, d * L : (d + 1) * L],
-            (middles[d] * gmix[d, 1:2, :]).astype(BF16),
+    parts = [(middles[d] * gmix[d, 1:2, :]).astype(BF16) for d in range(Y)]
+    part = jnp.concatenate(parts, axis=1)
+    fz = 4 * L // Z
+    for lo, hi, zs in ((2, 6, (4, 3, 5, 2)), (6, 8, (6, 7)), (0, 2, (1, 0))):
+        up = lax.dot_general(
+            wut[lo * fz : hi * fz, :],
+            part,
             (((1,), (1,)), ((), ())),
             preferred_element_type=F32,
         )
-    u6[...] = up.astype(BF16).reshape(Z, 4 * L // Z, B)
-    for zz in (4, 3, 5, 2, 6, 1, 7, 0):
-        @pl.when(z != zz)
-        def _(zz=zz):
-            put(u6.at[zz], r6.at[z], 11, (zz * Y + y, tp))
+        u6[lo:hi] = up.astype(BF16).reshape(hi - lo, fz, B)
+        for zz in zs:
+            @pl.when(z != zz)
+            def _(zz=zz):
+                put(u6.at[zz], r6.at[z], 11, (zz * Y + y, tp))
 
     r6[z] = u6[z]
     def down_rows(yy):
@@ -507,13 +503,14 @@
             ).astype(BF16)
     got(hall7.at[pl.ds(0, Z - 1)], 13)
     hid = hall7[...].reshape(4 * L, B)
-    for yy in (0, 1, 3, 2):
-        down = jnp.dot(wdt[yy * L : (yy + 1) * L, :], hid, preferred_element_type=F32)
-        d8[yy * T : (yy + 1) * T] = down.reshape(T, DT, B).astype(BF16)
-        for t in (1, 0, 3, 2, 7, 6, 5, 4):
-            @pl.when(me_p != yy * T + t)
-            def _(yy=yy, t=t):
-                put(d8.at[yy * T + t], r8.at[me_p], 14, (z * Y + yy, t))
+    for lo, hi, ys in ((0, 1, (0,)), (1, Y, (1, 3, 2))):
+        down = jnp.dot(wdt[lo * L : hi * L, :], hid, preferred_element_type=F32)
+        d8[lo * T : hi * T] = down.reshape((hi - lo) * T, DT, B).astype(BF16)
+        for yy in ys:
+            for t in (1, 0, 3, 2, 7, 6, 5, 4):
+                @pl.when(me_p != yy * T + t)
+                def _(yy=yy, t=t):
+                    put(d8.at[yy * T + t], r8.at[me_p], 14, (z * Y + yy, t))
 
     r8[me_p] = d8[me_p]
     got(sq.at[pl.ds(0, Z - 1)], 12)
@@ -532,9 +529,10 @@
 
 
 def hand_over(layer_in, state_in, layer_ref, state_ref, sems):
-    copies = [pltpu.make_async_copy(layer_in, layer_ref, sems.at[4])]
-    for r in range(ROWS):
-        copies.append(pltpu.make_async_copy(state_in.at[r], state_ref.at[r], sems.at[r]))
+    copies = [
+        pltpu.make_async_copy(state_in, state_ref, sems.at[0]),
+        pltpu.make_async_copy(layer_in, layer_ref, sems.at[1]),
+    ]
     for c in copies:
         c.start()
     for c in copies:
@@ -655,7 +653,7 @@
         ),
         in_specs=[anywhere] * 2,
         out_specs=(hbm, hbm),
-        scratch_shapes=[pltpu.SemaphoreType.DMA((5,))],
+        scratch_shapes=[pltpu.SemaphoreType.DMA((2,))],
         compiler_params=pltpu.CompilerParams(vmem_limit_bytes=2**20),
     )(layer_out, memory_next)
     return layer_out.T, memory_next

time: 58.2 us -> 57.3 us (0.985)
  Pallas kernels: 57.5 us -> 56.6 us
    pallas_call x1, Pallas kernels: 56.5 us -> 55.6 us  [shards(): pl.pallas_call(functools.partial(layer_kernel, Z, T), out_shape=(pltpu.VM...]
where the time goes in v7:
time: 57.3 us; the launch traced here: 57.2 us
  Pallas kernels  56.6 us (99%)
  between operations  0.64 us (1%)
    pallas_call x1, Pallas kernels, shards(): pl.pallas_call(functools.partial(layer_kernel, Z, T), out_shape=(pltpu.VM...  55.6 us

profile of v7, /device:TPU:1, one launch (start us, length us, event | category | flops | bytes accessed | tf_op | source)
XLA Modules:
  0.0 57.2 jit_solution(4329410459134746625)
XLA Ops:
  0.6 55.6 %shard_map.167 = (bf16[16,128]{1,0:T(8,128)(2,1)S(1)}, f32[4,4,128,128]{3,2,1,0:T(8,128)S(1)}) custom-call(bf16[16,128]{1,0:T(8,128)(2,1)} %bitcast.7, f32[1,128]{1,0:T(1,128)} %bitcast.10, f32[1,128]{1,0:T(1,128)} %bitcast.11, f32[1,128]{1,0:T(1,128)} %bitcast.12, bf16[4,128]{1,0:T(4,128)(2,1)} %bitcast.8, bf16[4,128]{1,0:T(4,128)(2,1)} %bitcast.9, ...), custom_call_target="tpu_custom_call" | custom-call | tf_op jit(solution)/shard_map/pallas_call | solution.py:576
  56.2 1.0 %shard_map.168 = (bf16[16,128]{1,0:T(8,128)(2,1)}, f32[4,4,128,128]{3,2,1,0:T(8,128)}) custom-call(bf16[16,128]{1,0:T(8,128)(2,1)S(1)} %get-tuple-element.6.layer_in, f32[4,4,128,128]{3,2,1,0:T(8,128)S(1)} %get-tuple-element.7.state_in), custom_call_target="tpu_custom_call" | custom-call | tf_op jit(solution)/shard_map/pallas_call | solution.py:648

commit v8 on v7

--- a/solution.py
+++ b/solution.py
@@ -74,7 +74,7 @@
     xz,
     s2,
     r2,
-    rows_f,
+    sb,
     hall,
     a4,
     r4,
@@ -317,14 +317,15 @@
         mine = jnp.where(lane_group == m, rolled, mine)
     cols = transposed(jnp.concatenate([mine, jnp.zeros((L - 16, B), F32)], axis=0))[0:16]
 
-    head_of = lax.div(lax.broadcasted_iota(jnp.int32, (16, L), 0), 4)
-    lane16 = lax.broadcasted_iota(jnp.int32, (16, L), 1)
-    beta16 = jnp.sum(jnp.where(lane16 == head_of, cols, 0.0), axis=1, keepdims=True)
-    decay16 = jnp.sum(jnp.where(lane16 == 4 + head_of, cols, 0.0), axis=1, keepdims=True)
+    pieces = [(h, r) for h in range(HEADS_DEV) for r in range(ROWS)]
+    load_state.wait()
+    for h, r in pieces:
+        tall, wide = h // 2 * L, h % 2 * L
+        sb[r, tall : tall + L, wide : wide + L] = state[r, h].astype(BF16)
+    row8 = lax.broadcasted_iota(jnp.int32, (8, L), 0)
+    row_of = lax.rem(row8, 4)
 
     got(r2.at[pl.ds(0, N - 1)], 5)
-    load_state.wait()
-    row_id = lax.broadcasted_iota(jnp.int32, (16, 1), 0)
     acts = []
     for h in range(HEADS_DEV):
         here = [
@@ -333,29 +334,35 @@
         qk = [r2[n, 0:8, :].astype(F32) for n in here[0]]
         vg = [r2[n, 8:16, :].astype(F32) for n in here[1]]
         total = jnp.concatenate([added(qk), added(vg)], axis=0)
-        a = silu(total * cols[:, 8:9])
-        inv = lax.rsqrt(jnp.sum(a * a, axis=1, keepdims=True) + EPS)
-        norm = jnp.where(row_id < 4, inv * L ** (-0.5), jnp.where(row_id < 8, inv, 1.0))
-        acts.append(a * norm)
-        for n, lo in ((0, 0), (1, 4), (2, 8), (3, 12)):
-            rows_f[n, 4 * h : 4 * h + 4, :] = acts[h][lo : lo + 4]
-    flipped = transposed(jnp.concatenate(acts + [jnp.zeros((L - 64, L), F32)], axis=0))
-    pieces = [(h, r) for h in range(HEADS_DEV) for r in range(ROWS)]
-    for h, r in pieces:
-        at = h * 16 + r
-        own = state[r, h]
-        row = 4 * h + r
-        rows_f[4, row : row + 1, :] = jnp.sum(
-            own * flipped[:, at : at + 1], axis=0, keepdims=True
-        )
-        rows_f[5, row : row + 1, :] = jnp.sum(
-            own * flipped[:, at + 4 : at + 5], axis=0, keepdims=True
-        )
-    corr = beta16 * (rows_f[2] - decay16 * rows_f[5])
-    along = jnp.sum(rows_f[0] * rows_f[1], axis=1, keepdims=True)
-    readout = decay16 * rows_f[4] + along * corr
-    readout = readout * lax.rsqrt(jnp.mean(readout * readout, axis=1, keepdims=True) + EPS)
-    hall[z] = (readout * head_gain_ref[...] * rows_f[3]).astype(BF16)
+        acts.append(silu(total * cols[:, 8:9]))
+    none = jnp.zeros((8, L), F32)
+    lhs = [
+        jnp.concatenate([acts[h][0:8], none] if h < 2 else [none, acts[h][0:8]], axis=1)
+        for h in range(HEADS_DEV)
+    ]
+    lhs = jnp.concatenate(lhs, axis=0).astype(BF16)
+    taken = [jnp.dot(lhs, sb[r], preferred_element_type=F32) for r in range(ROWS)]
+    corrs, gated = [], []
+    for h in range(HEADS_DEV):
+        wide = h % 2 * L
+        got_qk = taken[3][8 * h : 8 * h + 8, wide : wide + L]
+        for r in range(3):
+            got_qk = jnp.where(row_of == r, taken[r][8 * h : 8 * h + 8, wide : wide + L], got_qk)
+        q_rows, v_rows = acts[h][0:8], acts[h][8:16]
+        k_rows, gates = pltpu.roll(q_rows, 4, 0), pltpu.roll(v_rows, 4, 0)
+        q_norm = lax.rsqrt(jnp.sum(q_rows * q_rows, axis=1, keepdims=True) + EPS) * L ** (-0.5)
+        k_norm = lax.rsqrt(jnp.sum(k_rows * k_rows, axis=1, keepdims=True) + EPS)
+        along = jnp.sum(q_rows * k_rows, axis=1, keepdims=True) * (q_norm * k_norm)
+        beta, decay = cols[0:8, h : h + 1], cols[0:8, 4 + h : 5 + h]
+        corr = beta * (v_rows - (decay * k_norm) * pltpu.roll(got_qk, 4, 0))
+        readout = (decay * q_norm) * got_qk + along * corr
+        readout = readout * lax.rsqrt(jnp.mean(readout * readout, axis=1, keepdims=True) + EPS)
+        gated.append(readout * head_gain_ref[...] * gates)
+        corrs.append(k_norm * corr)
+    gated = [
+        jnp.where(row8 < 4, gated[h], pltpu.roll(gated[h + 1], 4, 0)) for h in (0, 2)
+    ]
+    hall[z] = jnp.concatenate(gated, axis=0).astype(BF16)
 
     offs = (4, 3, 5, 2, 6, 1, 7)
     for zz in (0, 1, 7, 2, 6, 3, 5, 4):
@@ -374,11 +381,12 @@
         put(up_cols(yy), wu.at[y], 6, (z * Y + yy, tp))
 
     got(sgath.at[7], 18)
+    flipped = transposed(jnp.concatenate(acts + [jnp.zeros((L - 64, L), F32)], axis=0))
     for h, r in pieces:
-        row = 4 * h + r
         at = h * 16 + 4 + r
         next_ref[r, h] = (
-            state[r, h] * decay16[row : row + 1] + flipped[:, at : at + 1] * corr[row : row + 1]
+            state[r, h] * cols[r : r + 1, 4 + h : 5 + h]
+            + flipped[:, at : at + 1] * corrs[h][r : r + 1]
         )
     row_mid = (tp * Y + y) * ROWS
     sel_row = lax.broadcasted_iota(jnp.int32, (16, B), 0)
@@ -600,7 +608,7 @@
             pltpu.VMEM((Z, 16, B), BF16),
             pltpu.VMEM((N // 2, 2, 16, L), BF16),
             pltpu.VMEM((N, 16, L), BF16),
-            pltpu.VMEM((6, 16, L), F32),
+            pltpu.VMEM((ROWS, 2 * L, 2 * L), BF16),
             pltpu.VMEM((Z, 16, L), BF16),
             pltpu.VMEM((Z // 2, 2, 16, L), BF16),
             pltpu.VMEM((T, 16, L), BF16),

time: 57.3 us -> 56.9 us (level)
  no operation moved by 1% of the time
where the time goes in v8:
time: 56.9 us; the launch traced here: 56.8 us
  Pallas kernels  56.2 us (99%)
  between operations  0.64 us (1%)
    pallas_call x1, Pallas kernels, shards(): pl.pallas_call(functools.partial(layer_kernel, Z, T), out_shape=(pltpu.VM...  55.2 us

profile of v8, /device:TPU:1, one launch (start us, length us, event | category | flops | bytes accessed | tf_op | source)
XLA Modules:
  0.0 56.8 jit_solution(17533079087024177886)
XLA Ops:
  0.6 55.2 %shard_map.167 = (bf16[16,128]{1,0:T(8,128)(2,1)S(1)}, f32[4,4,128,128]{3,2,1,0:T(8,128)S(1)}) custom-call(bf16[16,128]{1,0:T(8,128)(2,1)} %bitcast.7, f32[1,128]{1,0:T(1,128)} %bitcast.10, f32[1,128]{1,0:T(1,128)} %bitcast.11, f32[1,128]{1,0:T(1,128)} %bitcast.12, bf16[4,128]{1,0:T(4,128)(2,1)} %bitcast.8, bf16[4,128]{1,0:T(4,128)(2,1)} %bitcast.9, ...), custom_call_target="tpu_custom_call" | custom-call | tf_op jit(solution)/shard_map/pallas_call | solution.py:584
  55.9 1.0 %shard_map.168 = (bf16[16,128]{1,0:T(8,128)(2,1)}, f32[4,4,128,128]{3,2,1,0:T(8,128)}) custom-call(bf16[16,128]{1,0:T(8,128)(2,1)S(1)} %get-tuple-element.6.layer_in, f32[4,4,128,128]{3,2,1,0:T(8,128)S(1)} %get-tuple-element.7.state_in), custom_call_target="tpu_custom_call" | custom-call | tf_op jit(solution)/shard_map/pallas_call | solution.py:656

commit v9 on v8

--- a/solution.py
+++ b/solution.py
@@ -291,8 +291,9 @@
 
     for t in tps:
         put(sgath.at[0, tp], sgath.at[7, tp], 18, (spot_far, t))
+    load_out.wait()
     for off in (2, 1, 3):
-        put(wo_ref, own_out, 0, (z * Y + lax.rem(y + off, Y), tp))
+        put(own_out, own_out, 0, (z * Y + ys_[off], tp))
 
     for c in late:
         c.wait()
@@ -340,8 +341,12 @@
         jnp.concatenate([acts[h][0:8], none] if h < 2 else [none, acts[h][0:8]], axis=1)
         for h in range(HEADS_DEV)
     ]
-    lhs = jnp.concatenate(lhs, axis=0).astype(BF16)
-    taken = [jnp.dot(lhs, sb[r], preferred_element_type=F32) for r in range(ROWS)]
+    lhs = jnp.concatenate(lhs, axis=0)
+    high = lhs.astype(BF16)
+    low = (lhs - high.astype(F32)).astype(BF16)
+    both = jnp.concatenate([high, low], axis=0)
+    taken = [jnp.dot(both, sb[r], preferred_element_type=F32) for r in range(ROWS)]
+    taken = [part[0:32] + part[32:64] for part in taken]
     corrs, gated = [], []
     for h in range(HEADS_DEV):
         wide = h % 2 * L
@@ -401,7 +406,6 @@
             (((1,), (1,)), ((), ())),
             preferred_element_type=F32,
         )
-    load_out.wait()
     got(wof.at[:, pl.ds(0, 3 * L)], 0)
 
     got(hall.at[pl.ds(0, Z - 1)], 7)

time: 56.9 us -> 56.8 us (level)
  no operation moved by 1% of the time
where the time goes in v9:
time: 56.8 us; the launch traced here: 56.7 us
  Pallas kernels  56.1 us (99%)
  between operations  0.64 us (1%)
    pallas_call x1, Pallas kernels, shards(): pl.pallas_call(functools.partial(layer_kernel, Z, T), out_shape=(pltpu.VM...  55.1 us

profile of v9, /device:TPU:1, one launch (start us, length us, event | category | flops | bytes accessed | tf_op | source)
XLA Modules:
  0.0 56.7 jit_solution(1374728861016551993)
XLA Ops:
  0.6 55.1 %shard_map.167 = (bf16[16,128]{1,0:T(8,128)(2,1)S(1)}, f32[4,4,128,128]{3,2,1,0:T(8,128)S(1)}) custom-call(bf16[16,128]{1,0:T(8,128)(2,1)} %bitcast.7, f32[1,128]{1,0:T(1,128)} %bitcast.10, f32[1,128]{1,0:T(1,128)} %bitcast.11, f32[1,128]{1,0:T(1,128)} %bitcast.12, bf16[4,128]{1,0:T(4,128)(2,1)} %bitcast.8, bf16[4,128]{1,0:T(4,128)(2,1)} %bitcast.9, ...), custom_call_target="tpu_custom_call" | custom-call | tf_op jit(solution)/shard_map/pallas_call | solution.py:588
  55.7 1.0 %shard_map.168 = (bf16[16,128]{1,0:T(8,128)(2,1)}, f32[4,4,128,128]{3,2,1,0:T(8,128)}) custom-call(bf16[16,128]{1,0:T(8,128)(2,1)S(1)} %get-tuple-element.6.layer_in, f32[4,4,128,128]{3,2,1,0:T(8,128)S(1)} %get-tuple-element.7.state_in), custom_call_target="tpu_custom_call" | custom-call | tf_op jit(solution)/shard_map/pallas_call | solution.py:660
